TPU v7x, 128 devices: a whole 4x4x4 slice. The times are simulated.
128 devices in a mesh: sp: 16 (over z, x), dp: 8 (over y, core).
Axes of the slice: x: 4, y: 4, z: 4, core: 2. Of those that a mesh axis runs over, the one named last changes fastest.
Arguments:
- activations: bfloat16 [8, 8192, 2048], P('dp', 'sp'), may hold values from -6 to 6
- value_weight: bfloat16 [2048, 1024], P(('sp', 'dp')), may hold values from -0.125 to 0.125
- gate_weight: bfloat16 [2048, 1024], P(('sp', 'dp')), may hold values from -0.125 to 0.125
- input_weight: bfloat16 [2048, 512], P(('sp', 'dp')), may hold values from -0.125 to 0.125
- readout_weight: bfloat16 [2048, 512], P(('sp', 'dp')), may hold values from -0.125 to 0.125
- rate_weight: bfloat16 [2048, 16], replicated, may hold values from -0.125 to 0.125
- value_taps: bfloat16 [4, 1024], replicated, may hold values from -0.375 to 0.375
- input_taps: bfloat16 [4, 512], replicated, may hold values from -3 to 3
- readout_taps: bfloat16 [4, 512], replicated, may hold values from -3 to 3
- rate_bias: float32 [16], replicated, may hold values from -1 to 1
- decay_log: float32 [16], replicated, may hold values from -1 to 1.5
- norm_gain: float32 [1024], replicated, may hold values from 0.1 to 1.9
- out_weight: bfloat16 [1024, 2048], P(None, ('sp', 'dp')), may hold values from -0.1875 to 0.1875
Outputs:
- mixed_out: bfloat16 [8, 8192, 2048], P('dp', 'sp')
All inputs are finite; a program needn't handle non-finite values.
Results may differ from a plain program's by a relative error of at most 0.014.
Values may be sent and summed in bfloat16 or wider, within the bound.
A program may use at most 128 MiB of HBM per device.

v0:
```python
import jax
import jax.numpy as jnp
from jax import lax
from jax.sharding import PartitionSpec as P

HEADS = 16
HEAD_DIM = 64
GROUPS = 4
STATE = 128
CONV = 4
BLOCK = 64


norm_eps = 1.0


def sent_together(arrays, axis, dim, along):
    both = jnp.concatenate(arrays, axis=along)
    filled, at, finished = (lax.all_gather(both, axis, axis=dim, tiled=True), 0, [])
    for a in arrays:
        finished.append(lax.slice_in_dim(filled, at, at + a.shape[along], axis=along))
        at += a.shape[along]
    return tuple(finished)


def shifted(block, axis, distance):
    devices = range(lax.axis_size(axis))
    route = [(i - distance, i) for i in devices if i - distance in devices]
    return lax.ppermute(block, axis, route)


def sent_to_all(shard, axis):
    copies = jnp.broadcast_to(shard, (lax.axis_size(axis), *shard.shape))
    return lax.all_to_all(copies, axis, split_axis=0, concat_axis=0, tiled=True)


def combined_pairwise(pieces, combine):
    while len(jax.tree.leaves(pieces)[0]) > 1:
        pieces = jax.vmap(combine)(
            *(jax.tree.map(lambda part: part[side::2], pieces) for side in (0, 1))
        )
    return jax.tree.map(lambda part: part[0], pieces)


def carried_in(shard, axis, combine, identity):
    devices, index = (lax.axis_size(axis), lax.axis_index(axis))
    passed = jnp.arange(devices) < index

    def kept(part, zero, own):
        part = jnp.where(
            passed.reshape(-1, *(1 for _ in own.shape)),
            part.astype(own.dtype),
            jnp.asarray(zero, own.dtype),
        )
        return part

    pieces = jax.tree.map(
        lambda part: sent_to_all(part, axis),
        jax.tree.map(lambda part, kind: part.astype(kind), shard, (jnp.bfloat16, jnp.bfloat16)),
    )
    return combined_pairwise(jax.tree.map(kept, pieces, identity, shard), combine)


def broaden(matrix, groups, head_count):
    row_count = matrix.shape[0]
    group_width = matrix.shape[1] // groups
    spread = matrix.reshape(row_count, groups, 1, group_width)
    spread = jnp.broadcast_to(spread, (row_count, groups, head_count // groups, group_width))
    return spread.reshape(row_count, head_count * group_width)


def extended_conv(before, series, kernel):
    extent = kernel.shape[0]
    length = series.shape[0]
    padded = jnp.concatenate([before, series], axis=0).astype(jnp.float32)
    result = jnp.zeros(series.shape, jnp.float32)
    for offset in range(extent):
        result = result + kernel[offset].astype(jnp.float32) * padded[offset : offset + length]
    return result


def block_parts(values, inputs, readouts, rates, decay):
    length, head_count, head_width = values.shape
    blocks = length // BLOCK
    block_values = values.reshape(blocks, BLOCK, head_count, head_width)
    block_inputs = inputs.reshape(blocks, BLOCK, head_count, -1)
    block_reads = readouts.reshape(blocks, BLOCK, head_count, -1)
    block_rates = rates.reshape(blocks, BLOCK, head_count)
    running = jnp.cumsum(block_rates * decay, axis=1)
    by_head = jnp.transpose(running, (0, 2, 1))
    rate_head = jnp.transpose(block_rates, (0, 2, 1))
    causal = jnp.tril(jnp.ones((BLOCK, BLOCK), dtype=bool))
    intervals = by_head[:, :, :, None] - by_head[:, :, None, :]
    fading = jnp.where(causal, jnp.exp(jnp.minimum(intervals, 0.0)), 0.0)
    intersect = jnp.einsum(
        "bthn,bshn->bhts", block_reads, block_inputs, preferred_element_type=jnp.float32
    )
    scores = (intersect * fading * rate_head[:, :, None, :]).astype(jnp.bfloat16)
    within = jnp.einsum("bhts,bshp->bthp", scores, block_values, preferred_element_type=jnp.float32)
    tail_fade = jnp.exp(running[:, -1:, :] - running) * block_rates
    weighted = (block_values.astype(jnp.float32) * tail_fade[:, :, :, None]).astype(jnp.bfloat16)
    states = jnp.einsum(
        "bshp,bshn->bhpn", weighted, block_inputs, preferred_element_type=jnp.float32
    )
    return (within, states, running, block_reads)


def summarize(states, running):
    totals = jnp.cumsum(running[:, -1, :], axis=0)
    last = totals[-1]
    end_state = jnp.einsum(
        "dh,dhpn->hpn", jnp.exp(last[None, :] - totals), states, precision=lax.Precision.HIGHEST
    )
    return (end_state, last)


def finish(within, states, running, block_reads, initial):
    blocks, block_len, head_count, head_width = within.shape
    totals = jnp.cumsum(running[:, -1, :], axis=0)
    starts = totals - running[:, -1, :]
    earlier = jnp.tril(jnp.ones((blocks, blocks), dtype=bool), -1)
    carried = jnp.where(
        earlier[:, :, None], jnp.exp(jnp.minimum(starts[:, None, :] - totals[None, :, :], 0.0)), 0.0
    )
    entering = jnp.einsum("cdh,dhpn->chpn", carried, states, precision=lax.Precision.HIGHEST)
    entering = entering + jnp.exp(starts)[:, :, None, None] * initial[None]
    across = jnp.einsum(
        "bthn,bhpn->bthp",
        block_reads.astype(jnp.float32),
        entering,
        precision=lax.Precision.HIGHEST,
    )
    across = across * jnp.exp(running)[:, :, :, None]
    return (within + across).reshape(blocks * block_len, head_count * head_width)


def link(earlier, later):
    return (jnp.exp(later[1])[:, None, None] * earlier[0] + later[0], earlier[1] + later[1])


def per_device(
    activations,
    value_weight,
    gate_weight,
    input_weight,
    readout_weight,
    rate_weight,
    value_taps,
    input_taps,
    readout_taps,
    rate_bias,
    decay_log,
    norm_gain,
    out_weight,
):
    sequence = activations[0]
    row_count = sequence.shape[0]

    def add_rows(piece):
        return jnp.dot(sequence, piece, preferred_element_type=jnp.float32)

    rate_raw = jnp.dot(sequence, rate_weight, preferred_element_type=jnp.float32).astype(
        jnp.bfloat16
    )
    pieces = sent_together(
        (value_weight, gate_weight, input_weight, readout_weight), ("sp", "dp"), 0, 1
    )
    value_sum, gate_sum, input_sum, readout_sum = tuple((add_rows(piece) for piece in pieces))
    gate_proj = gate_sum.astype(jnp.bfloat16)
    own_values = value_sum.astype(jnp.bfloat16)
    own_inputs = input_sum.astype(jnp.bfloat16)
    own_reads = readout_sum.astype(jnp.bfloat16)
    edge = CONV - 1
    joined = jnp.concatenate(
        [
            own_values[row_count - edge :],
            own_inputs[row_count - edge :],
            own_reads[row_count - edge :],
        ],
        axis=1,
    )
    before = shifted(joined, "sp", 1)
    split_one = own_values.shape[1]
    split_two = split_one + own_inputs.shape[1]
    conv_values = jax.nn.silu(extended_conv(before[:, :split_one], own_values, value_taps)).astype(
        jnp.bfloat16
    )
    conv_inputs = jax.nn.silu(
        extended_conv(before[:, split_one:split_two], own_inputs, input_taps)
    ).astype(jnp.bfloat16)
    conv_reads = jax.nn.silu(extended_conv(before[:, split_two:], own_reads, readout_taps)).astype(
        jnp.bfloat16
    )
    head_inputs = broaden(conv_inputs, GROUPS, HEADS).reshape(row_count, HEADS, STATE)
    head_reads = broaden(conv_reads, GROUPS, HEADS).reshape(row_count, HEADS, STATE)
    rates = jax.nn.softplus(rate_raw.astype(jnp.float32) + rate_bias)
    decay = -jnp.exp(decay_log) / (row_count * lax.axis_size("sp"))
    within, states, running, block_reads = block_parts(
        conv_values.reshape(row_count, HEADS, HEAD_DIM), head_inputs, head_reads, rates, decay
    )
    end_state, end_total = summarize(states, running)
    prior_state, prior_total = carried_in(
        (end_state, end_total), "sp", link, (jnp.zeros_like(end_state), jnp.zeros_like(end_total))
    )
    returned = finish(within, states, running, block_reads, prior_state).astype(jnp.bfloat16)
    gated = returned.astype(jnp.float32) * jax.nn.silu(gate_proj.astype(jnp.float32))
    scale = lax.rsqrt(jnp.mean(gated * gated, axis=-1, keepdims=True) + norm_eps)
    normed = (gated * scale * norm_gain).astype(jnp.bfloat16)
    result = jnp.dot(
        normed,
        lax.all_gather(out_weight, ("sp", "dp"), axis=1, tiled=True),
        preferred_element_type=jnp.float32,
    )
    return result.astype(jnp.bfloat16)[None]


def solution(mesh):
    placed = (
        P("dp", "sp", None),
        P(("sp", "dp"), None),
        P(("sp", "dp"), None),
        P(("sp", "dp"), None),
        P(("sp", "dp"), None),
        P(),
        P(),
        P(),
        P(),
        P(),
        P(),
        P(),
        P(None, ("sp", "dp")),
    )
    return jax.shard_map(
        per_device, mesh=mesh, in_specs=placed, out_specs=P("dp", "sp", None), check_vma=False
    )
```

profile of v0, /device:TPU:0, one launch (start us, length us, event | category | flops | bytes accessed | tf_op | source)
XLA Modules:
  0.0 257.3 jit_solution(12794118743103291800)
XLA Ops:
  6.5 1.6 pad_maximum_fusion
  8.2 0.0 copy-done
  8.2 1.5 compare_select_fusion
  9.7 0.1 reshape.86
  9.8 0.2 copy.44
  10.0 0.1 fusion.102
  10.1 0.6 broadcast_in_dim.61
  10.7 8.0 %all-to-all-start = ((bf16[16,1,16]{2,1,0:T(2,128)(2,1)}), bf16[16,1,16]{2,1,0:T(2,128)(2,1)}, u32[]{:S(2)}, u32[]{:S(2)}) async-start(bf16[16,1,16]{2,1,0:T(2,128)(2,1)} %broadcast_in_dim.61), calls=%async_computation | async-start | bytes 16384 | tf_op jit(solution)/shard_map/all_to_all | solution.py:34
  18.8 0.6 subtract_exponential_fusion
  19.4 0.6 slice_convert_fusion.3
  20.0 0.9 exponential_multiply_fusion
  20.9 65.2 %all-gather.3.cloned.1.call-done = bf16[2048,3072]{1,0:T(8,128)(2,1)} async-done(((bf16[16,3072]{1,0:T(8,128)(2,1)}), bf16[2048,3072]{1,0:T(8,128)(2,1)}) %all-gather.3.cloned.1.call-update) | async-done | bytes 12582928 | tf_op jit(solution)/shard_map/all_gather | solution.py:19
  86.1 4.5 %fusion.53 = bf16[512,1024]{1,0:T(8,128)(2,1)S(1)} fusion(bf16[2048,3072]{1,0:T(8,128)(2,1)} %all-gather.3.cloned.1.call-done, bf16[1,512,2048]{2,1,0:T(8,128)(2,1)S(1)} %copy-done), kind=kOutput, calls=%fused_computation.56 | convolution fusion | flops 2148007936 | bytes 7340032 | tf_op jit(solution)/shard_map/dot_general | solution.py:160
  90.6 2.8 %fusion.73 = bf16[512,512]{1,0:T(8,128)(2,1)S(1)} fusion(bf16[2048,3072]{1,0:T(8,128)(2,1)} %all-gather.3.cloned.1.call-done, bf16[1,512,2048]{2,1,0:T(8,128)(2,1)S(1)} %copy-done), kind=kOutput, calls=%fused_computation.60 | convolution fusion | flops 1074003968 | bytes 4718592 | tf_op jit(solution)/shard_map/dot_general | solution.py:160
  93.5 3.0 %fusion.68 = bf16[512,512]{1,0:T(8,128)(2,1)S(1)} fusion(bf16[2048,3072]{1,0:T(8,128)(2,1)} %all-gather.3.cloned.1.call-done, bf16[1,512,2048]{2,1,0:T(8,128)(2,1)S(1)} %copy-done), kind=kOutput, calls=%fused_computation.59 | convolution fusion | flops 1074003968 | bytes 4718592 | tf_op jit(solution)/shard_map/dot_general | solution.py:160
  96.5 0.8 copy-done.8
  97.3 0.6 pad_maximum_fusion.1
  97.9 3.9 %collective-permute-start = (bf16[3,2048]{1,0:T(4,128)(2,1)}, bf16[3,2048]{1,0:T(4,128)(2,1)}, u32[]{:S(2)}, u32[]{:S(2)}) collective-permute-start(bf16[3,2048]{1,0:T(4,128)(2,1)} %pad_maximum_fusion.1), channel_id=1, source_target_pairs={{0,8},{8,16},{16,24},{24,32},{32,40},{40,48},{48,56},{56,64},{64,7... | collective-permute-start | bytes 36872 | tf_op jit(solution)/shard_map/ppermute | solution.py:29
  101.9 0.6 slice_convert_fusion.7
  102.5 1.1 copy.51
  103.5 1.4 copy.63
  104.9 0.7 slice.216
  105.6 0.3 maximum_convert_fusion
  105.9 2.0 multiply_convert_fusion.4
  107.9 2.3 reshape_reshape.3
  110.2 4.5 %copy.48 = bf16[8,64,16,64]{1,3,2,0:T(8,128)(2,1)} copy(bf16[8,64,16,64]{3,2,1,0:T(8,128)(2,1)} %reshape_reshape.3) | data formatting | bytes 2097152 | tf_op jit(solution)/shard_map/reshape;reshape | solution.py:85
  114.7 0.7 fusion.120
  115.4 1.4 maximum_convert_fusion.1
  116.8 0.7 copy_bitcast_fusion
  117.5 0.4 broadcast_in_dim.57
  117.9 1.7 copy-done.5
  119.6 0.7 fusion.15
  120.3 5.2 %fusion.8 = f32[16,1,64,128]{3,1,2,0:T(1,128)S(1)} fusion(f32[8,16,1,1]{0,2,3,1:T(1,128)S(1)} %copy-done.12, f32[8,16,64,128]{3,2,1,0:T(8,128)S(1)} %fusion.15), kind=kOutput, calls=%fused_computation.14 | convolution fusion | flops 12582912 | bytes 4719104 | tf_op jit(solution)/shard_map/dh,dhpn->hpn/dot_general | solution.py:111
  125.6 0.8 convert_element_type.137
  126.3 4.0 %broadcast_in_dim.68 = bf16[16,16,64,128]{3,2,1,0:T(8,128)(2,1)} broadcast(bf16[16,64,128]{2,1,0:T(8,128)(2,1)} %convert_element_type.137), dimensions={1,2,3} | broadcast | bytes 4456448 | tf_op jit(solution)/shard_map/broadcast_in_dim | solution.py:33
  130.4 5.9 %all-to-all-start.1 = ((bf16[16,16,64,128]{3,2,1,0:T(8,128)(2,1)}), bf16[16,16,64,128]{3,2,1,0:T(8,128)(2,1)}, u32[]{:S(2)}, u32[]{:S(2)}) async-start(bf16[16,16,64,128]{3,2,1,0:T(8,128)(2,1)} %broadcast_in_dim.68), calls=%async_computation.1 | async-start | bytes 8388608 | tf_op jit(solution)/shard_map/all_to_all | solution.py:34
  136.3 0.3 all-gather.5.cloned.1.call-start
  136.6 0.5 all-gather.5.cloned.1.call-update
  137.1 0.7 copy.54
  137.7 0.6 copy.91
  138.4 0.7 copy.56
  139.0 0.7 copy.53
  139.7 1.1 copy.59
  140.8 0.1 copy.45
  140.9 0.1 iota_compare_fusion.1
  141.0 0.8 slice_convert_fusion.11
  141.8 0.7 convert_element_type.147
  142.6 0.1 broadcast_select_fusion
  142.8 1.5 copy_bitcast_fusion.1
  144.3 55.6 %all-to-all-done.1 = bf16[16,16,64,128]{3,2,1,0:T(8,128)(2,1)} async-done(((bf16[16,16,64,128]{3,2,1,0:T(8,128)(2,1)}), bf16[16,16,64,128]{3,2,1,0:T(8,128)(2,1)}, u32[]{:S(2)}, u32[]{:S(2)}) %all-to-all-start.1) | async-done | bytes 4194336 | tf_op jit(solution)/shard_map/all_to_all | solution.py:34
  199.9 3.6 %convert_select_fusion = f32[16,16,64,128]{3,2,1,0:T(8,128)S(1)} fusion(bf16[16,16,64,128]{3,2,1,0:T(8,128)(2,1)} %all-to-all-done.1, pred[16]{0:T(512)(128)(4,1)S(1)} %iota_compare_fusion.2), kind=kLoop, calls=%fused_computation | loop fusion | flops 4194304 | bytes 12582928 | tf_op jit(solution)/shard_map/jit(_where)/select_n | solution.py:50
  203.6 0.5 slice_add_fusion
  204.1 0.3 slice_add_fusion.1
  204.4 0.2 slice_add_fusion.2
  204.5 0.1 fusion.99
  204.7 1.9 copy-done.2
  206.5 6.9 %bitcast_add_fusion = f32[8,16,64,128]{3,0,2,1:T(8,128)S(1)} fusion(f32[8,16,64,128]{3,2,1,0:T(8,128)S(1)} %copy-done.2, f32[16,64,128]{2,1,0:T(8,128)S(1)} %fusion.99, f32[8,16]{0,1:T(8,128)S(1)} %copy-done.15, f32[8,16]{0,1:T(8,128)S(1)} %copy-done.14, f32[8,16]{0,1:T(8,128)S(1)} %copy-done.16, pred[8,8]{1,0:T(8,128)(4,1)S(1)} %iota_compare_fusion.1), kind=kOutput, calls=%fused_computation.8 | convolution fusion | flops 102763520 | bytes 8914496 | tf_op jit(solution)/shard_map/cdh,dhpn->chpn/dot_general | solution.py:125
  213.4 0.4 broadcast_in_dim.54
  213.8 5.4 %fusion.6 = f32[8,16,64,64]{3,2,1,0:T(8,128)} fusion(f32[8,16,64,128]{3,0,2,1:T(8,128)S(1)} %bitcast_add_fusion, bf16[8,64,16,128]{3,1,0,2:T(8,128)(2,1)S(1)} %bitcast.136), kind=kOutput, calls=%fused_computation.9 | convolution fusion | flops 805306368 | bytes 8388608 | tf_op jit(solution)/shard_map/bthn,bhpn->bthp/dot_general | solution.py:127
  219.3 7.0 %fusion.34 = f32[8,64,16,64]{1,3,2,0:T(8,128)} fusion(f32[8,64,16]{1,2,0:T(8,128)S(1)} %copy.59, f32[8,16,64,64]{3,2,1,0:T(8,128)} %fusion.6, bf16[8,64,16,64]{1,3,2,0:T(8,128)(2,1)} %copy.48, f32[8,16,64]{2,1,0:T(8,128)S(1)} %bitcast.142, f32[8,16,64]{2,1,0:T(8,128)S(1)} %copy.45, pred[64,64]{1,0:T(8,128)(4,1)S(1)} %iota_compare_fusion, ...), kind=kOutput, calls=%fused_computation.49 | convolution fusion | flops 206569472 | bytes 9539584 | tf_op jit(solution)/shard_map/bhts,bshp->bthp/dot_general | solution.py:99
  226.3 5.8 %copy.60 = f32[8,64,16,64]{3,2,1,0:T(8,128)} copy(f32[8,64,16,64]{1,3,2,0:T(8,128)} %fusion.34) | data formatting | bytes 4194304 | tf_op jit(solution)/shard_map/convert_element_type | solution.py:206
  232.1 4.8 %reshape.100 = f32[512,1024]{1,0:T(8,128)} reshape(f32[8,64,16,64]{3,2,1,0:T(8,128)} %copy.60) | data formatting | bytes 4194304 | tf_op jit(solution)/shard_map/convert_element_type | solution.py:206
  237.0 6.9 %multiply_reduce_fusion = (f32[512]{0:T(512)S(1)}, f32[512,1024]{1,0:T(8,128)}) fusion(f32[512,1024]{1,0:T(8,128)} %reshape.100, bf16[2048,3072]{1,0:T(8,128)(2,1)} %all-gather.3.cloned.1.call-done, bf16[1,512,2048]{2,1,0:T(8,128)(2,1)S(1)} %copy-done), kind=kOutput, calls=%fused_computation.45 | convolution fusion | flops 2152201728 | bytes 10487808 | tf_op jit(solution)/shard_map/dot_general | solution.py:160
  243.9 6.5 %fusion.12 = bf16[1,512,2048]{2,1,0:T(8,128)(2,1)} fusion(bf16[1024,2048]{0,1:T(8,128)(2,1)} %all-gather.5.cloned.1.call-done, f32[512,1024]{1,0:T(8,128)} %get-tuple-element.30, f32[1024]{0:T(1024)S(1)} %copy-done.23, f32[512]{0:T(512)S(1)} %add_rsqrt_fusion), kind=kOutput, calls=%fused_computation.19 | convolution fusion | flops 2150105088 | bytes 8394752 | tf_op jit(solution)/shard_map/dot_general | solution.py:209
  (74 shorter events, 0.4 us)
Async XLA Ops:
  6.5 1.7 copy-start
  6.5 3.4 %copy-start.24 = (f32[16]{0:T(128)S(1)}, f32[16]{0:T(128)}, u32[]{:S(2)}) copy-start(f32[16]{0:T(128)} %param.23) | copy-start | bytes 196
  6.5 12.8 %copy-start.13 = (bf16[4,1024]{1,0:T(4,128)(2,1)S(1)}, bf16[4,1024]{1,0:T(4,128)(2,1)}, u32[]{:S(2)}) copy-start(bf16[4,1024]{1,0:T(4,128)(2,1)} %param.19) | copy-start | bytes 24580
  6.5 79.5 %all-gather.3.cloned.1.call-start = ((), (), s32[]{:S(2)}) async-start(), calls=%async_computation.2 | async-start | bytes 12681216 | tf_op jit(solution)/shard_map/all_gather | solution.py:19
  10.1 10.8 %copy-start.9 = (f32[8,16]{1,0:T(8,128)}, f32[8,16]{1,0:T(8,128)S(1)}, u32[]{:S(2)}) copy-start(f32[8,16]{1,0:T(8,128)S(1)} %reduce_window_sum.26) | copy-start | bytes 1540
  10.7 115.6 %all-to-all-start = ((bf16[16,1,16]{2,1,0:T(2,128)(2,1)}), bf16[16,1,16]{2,1,0:T(2,128)(2,1)}, u32[]{:S(2)}, u32[]{:S(2)}) async-start(bf16[16,1,16]{2,1,0:T(2,128)(2,1)} %broadcast_in_dim.61), calls=%async_computation | async-start | bytes 16384 | tf_op jit(solution)/shard_map/all_to_all | solution.py:34
  93.4 3.1 %copy-start.7 = (bf16[512,512]{1,0:T(8,128)(2,1)}, bf16[512,512]{1,0:T(8,128)(2,1)S(1)}, u32[]{:S(2)}) copy-start(bf16[512,512]{1,0:T(8,128)(2,1)S(1)} %fusion.73) | copy-start | bytes 1572868
  93.5 8.4 %copy-start.17 = (bf16[4,512]{1,0:T(4,128)(2,1)S(1)}, bf16[4,512]{1,0:T(4,128)(2,1)}, u32[]{:S(2)}) copy-start(bf16[4,512]{1,0:T(4,128)(2,1)} %param.20) | copy-start | bytes 12292
  96.5 0.8 copy-start.8
  97.9 6.9 %collective-permute-start = (bf16[3,2048]{1,0:T(4,128)(2,1)}, bf16[3,2048]{1,0:T(4,128)(2,1)}, u32[]{:S(2)}, u32[]{:S(2)}) collective-permute-start(bf16[3,2048]{1,0:T(4,128)(2,1)} %pad_maximum_fusion.1), channel_id=1, source_target_pairs={{0,8},{8,16},{16,24},{24,32},{32,40},{40,48},{48,56},{56,64},{64,7... | collective-permute-start | bytes 36872 | tf_op jit(solution)/shard_map/ppermute | solution.py:29
  114.7 2.1 copy-start.19
  114.7 2.1 copy-start.20
  114.7 2.1 copy-start.21
  114.7 2.1 copy-start.22
  117.5 2.1 copy-start.5
  117.9 2.4 copy-start.4
  119.6 0.7 copy-start.12
  120.3 5.2 %copy-start.1 = (f32[8,16,64,128]{3,2,1,0:T(8,128)}, f32[8,16,64,128]{3,2,1,0:T(8,128)S(1)}, u32[]{:S(2)}) copy-start(f32[8,16,64,128]{3,2,1,0:T(8,128)S(1)} %fusion.15) | copy-start | bytes 12582916
  130.4 6.7 %copy-start.10 = (f32[8,16]{1,0:T(8,128)S(1)}, f32[8,16]{1,0:T(8,128)}, u32[]{:S(2)}) copy-start(f32[8,16]{1,0:T(8,128)} %copy-done.9) | copy-start | bytes 1540
  130.4 8.0 %copy-start.18 = (f32[8,16]{1,0:T(8,128)S(1)}, f32[8,16]{1,0:T(8,128)}, u32[]{:S(2)}) copy-start(f32[8,16]{1,0:T(8,128)} %get-tuple-element.17) | copy-start | bytes 1540
  130.4 69.6 %all-to-all-start.1 = ((bf16[16,16,64,128]{3,2,1,0:T(8,128)(2,1)}), bf16[16,16,64,128]{3,2,1,0:T(8,128)(2,1)}, u32[]{:S(2)}, u32[]{:S(2)}) async-start(bf16[16,16,64,128]{3,2,1,0:T(8,128)(2,1)} %broadcast_in_dim.68), calls=%async_computation.1 | async-start | bytes 8388608 | tf_op jit(solution)/shard_map/all_to_all | solution.py:34
  136.3 107.6 %all-gather.5.cloned.1.call-start = ((), (), s32[]{:S(2)}) async-start(), calls=%async_computation.3 | async-start | bytes 4227072 | tf_op jit(solution)/shard_map/all_gather | solution.py:211
  204.3 2.2 copy-start.2
  204.3 2.2 copy-start.14
  204.3 2.2 copy-start.15
  204.4 2.2 copy-start.16
  206.5 6.9 %copy-start.6 = (bf16[512,4,128]{2,0,1:T(8,128)(2,1)S(1)}, bf16[512,4,128]{2,0,1:T(8,128)(2,1)}, u32[]{:S(2)}) copy-start(bf16[512,4,128]{2,0,1:T(8,128)(2,1)} %copy_bitcast_fusion.1) | copy-start | bytes 1572868
  213.8 5.5 %copy-start.3 = (bf16[512,4,4,128]{3,0,2,1:T(8,128)(2,1)}, bf16[512,4,4,128]{3,0,2,1:T(8,128)(2,1)S(1)}, u32[]{:S(2)}) copy-start(bf16[512,4,4,128]{3,0,2,1:T(8,128)(2,1)S(1)} %broadcast_in_dim.54) | copy-start | bytes 6291460
  213.8 5.4 %copy-start.11 = (f32[8,64,16]{1,2,0:T(8,128)S(1)}, f32[8,64,16]{1,2,0:T(8,128)}, u32[]{:S(2)}) copy-start(f32[8,64,16]{1,2,0:T(8,128)} %copy.91) | copy-start | bytes 98308
  237.0 6.9 %copy-start.23 = (f32[1024]{0:T(1024)S(1)}, f32[1024]{0:T(1024)}, u32[]{:S(2)}) copy-start(f32[1024]{0:T(1024)} %param.24) | copy-start | bytes 12292
Sparse Core Ops, SparseCore 0:
  10.5 75.5 all-gather.2
  140.2 92.5 all-gather.4
where the time goes:
time: 258 us; the launch traced here: 257 us
  waiting for transfers between devices  121 us (47%)
  matrix products  50.6 us (20%)
  local copies, waits for them, and re-layouts  35.3 us (14%)
  starting transfers between devices  18.1 us (7%)
  other arithmetic  18.1 us (7%)
  between operations  13.8 us (5%)
    all_gather x1, waiting for transfers between devices, sent_together(): lax.all_gather(both, axis, axis=dim, tiled=True)  65.2 us
    all_to_all x2, waiting for transfers between devices, sent_to_all(): return lax.all_to_all(copies, axis, split_axis=0, concat_axis=0, tiled=True)  55.6 us
    dot_general x4, matrix products, add_rows(): return jnp.dot(sequence, piece, preferred_element_type=jnp.float32)  17.3 us
    all_to_all x2, starting transfers between devices, sent_to_all(): return lax.all_to_all(copies, axis, split_axis=0, concat_axis=0, tiled=True)  14 us
    convert_element_type x2, local copies, waits for them, and re-layouts, per_device(): returned.astype(jnp.float32) * jax.nn.silu(gate_proj.astype(jnp.float32))  10.7 us
    dot_general x1, matrix products, block_parts(): jnp.einsum('bhts,bshp->bthp', scores, block_values, preferred_element_typ...  7.02 us
    dot_general x1, matrix products, finish(): jnp.einsum('cdh,dhpn->chpn', carried, states, precision=lax.Precision.HIG...  6.87 us
    another operation x2, local copies, waits for them, and re-layouts, block_parts(): block_values = values.reshape(blocks, BLOCK, head_count, head_width)  6.79 us
  transfers between devices with their start and end apart: 5, of which 2 were waited for; matrix products, arithmetic and copies ran while one was open for 34% of the time, Pallas kernels for 0%

commit v1 on v0

v1 whole, which is shorter than its diff:
```python
import jax
import jax.numpy as jnp
from jax import lax
from jax.experimental import pallas as pl
from jax.experimental.pallas import tpu as pltpu
from jax.sharding import PartitionSpec as P

F32 = jnp.float32
BF16 = jnp.bfloat16
MESH = pl.DeviceIdType.MESH

ROWS = 512
HALO = 16
LENGTH = 8192
WIDTH = 1024
BLOCK = 64
SPAN = 16

ORDER = (("x", "y", "z"), ("y", "z", "x"), ("z", "x", "y"))
STREAMS = ((0, 3), (3, 3), (6, 2))
VALUES, INPUTS, READS, GATE, OUT = (0, 3), 6, 1, (4, 7), (2, 5)


def silu(v):
    return (0.5 * v) * (1.0 + jnp.tanh(0.5 * v))


def rounded(v):
    return v.astype(BF16).astype(F32)


def split3(x):
    hi = x.astype(BF16)
    rest = x - hi.astype(F32)
    mid = rest.astype(BF16)
    return hi, mid, (rest - mid.astype(F32)).astype(BF16)


def dot(a, b):
    return jnp.dot(a, b, preferred_element_type=F32)


def spread(x, m):
    return sum(dot(part, m) for part in split3(x))


def kernel(
    act_hbm,
    wcat,
    rate_w,
    value_taps,
    input_taps,
    read_taps,
    bias,
    decay_log,
    gain,
    out,
    W,
    act,
    proj,
    rate_s,
    A,
    B,
    EM,
    VB,
    IT,
    R,
    SG,
    ST,
    EN,
    tb,
    tbuf,
    D,
    xs,
    rb,
    ps,
    pb,
    GT,
    NORM,
    ss,
    rs,
    ss2,
    rs2,
    ls,
):
    sp = lax.axis_index("sp")
    dp = lax.axis_index("dp")
    c = {"z": sp // 4, "x": sp % 4, "y": dp // 2}
    core = dp % 2
    other = 1 - core
    partner = (sp, c["y"] * 2 + other)

    def neighbour(d, step):
        at = dict(c)
        at[d] = (c[d] + step) % 4
        return at["z"] * 4 + at["x"], at["y"] * 2 + core

    load_act = pltpu.make_async_copy(act_hbm, act.at[pl.ds(HALO, ROWS)], ls.at[0])
    load_act.start()
    here = (c["z"], c["x"], c["y"])
    load_w = pltpu.make_async_copy(wcat.at[:, core], W.at[(slice(None), core, *here, core)], ls.at[1])
    load_w.start()

    barrier = pltpu.get_barrier_semaphore()

    def greet(d, carry):
        pl.semaphore_signal(barrier, inc=1, device_id=((sp + d) % SPAN, dp), device_id_type=MESH)
        return carry

    lax.fori_loop(1, SPAN, greet, 0)
    for peer in (neighbour("y", 1), neighbour("y", 3), partner):
        pl.semaphore_signal(barrier, inc=1, device_id=peer, device_id_type=MESH)
    pl.semaphore_wait(barrier, SPAN - 1 + 3)

    pending = []

    def copy(src, dst, k, device):
        return pltpu.make_async_remote_copy(
            src_ref=src,
            dst_ref=dst,
            send_sem=ss.at[k],
            recv_sem=rs.at[k],
            device_id=device,
            device_id_type=MESH,
        )

    def send(src, dst, k, device):
        started = copy(src, dst, k, device)
        started.start()
        pending.append(started)

    def arrived(dst, k):
        copy(dst, dst, k, partner).wait_recv()

    def piece(phase, color, first, count, index, half=None):
        dims = ORDER[color]
        at = dict(c)
        for d in dims[:phase]:
            at[d] = slice(None)
        at[dims[phase]] = index
        rows = slice(None)
        if half is not None:
            if phase == 0:
                rows = slice(half, half + 1)
            else:
                d = [d for d in "zxy" if d in dims[:phase]][0]
                at[d] = slice(2 * half, 2 * half + 2)
        return W.at[slice(first, first + count), core, at["z"], at["x"], at["y"], rows]

    def ring_start(phase, color, first, count, k):
        d = ORDER[color][phase]
        own = piece(phase, color, first, count, c[d])
        send(own, own, k, neighbour(d, 1))
        send(own, own, k + 1, neighbour(d, 3))

    def ring_pass(phase, color, first, count, k):
        d = ORDER[color][phase]
        for side, (back, ahead) in enumerate(((3, 1), (1, 3))):
            index = (c[d] + back) % 4
            arrived(piece(phase, color, first, count, index), k + side)
            half = piece(phase, color, first, count, index, side)
            send(half, half, k + 2 + side, neighbour(d, ahead))

    def ring_end(phase, color, first, count, k):
        index = (c[ORDER[color][phase]] + 2) % 4
        for side in range(2):
            arrived(piece(phase, color, first, count, index, side), k + 2 + side)

    def one(step, color):
        first, count = STREAMS[color]
        step(0, color, first, count, 4 * color)

    def two(step, stream):
        step(1, stream // 3, stream, 1, 12 + 4 * stream)

    def three(step, stream):
        step(2, stream // 3, stream, 1, 44 + 4 * stream)

    WAVES = ((0, 3, 6), (1, 4, 7), (2, 5))

    def share(stream):
        whole = W.at[stream, core]
        send(whole, whole, 76 + stream, partner)

    def shared(stream):
        arrived(W.at[stream, other], 76 + stream)

    SHARDS, EDGE = 84, 85

    def exchange_copy(q, src, dst, d):
        j = (sp + d) % SPAN
        return pltpu.make_async_remote_copy(
            src_ref=src(j),
            dst_ref=dst(sp),
            send_sem=ss2.at[q, d],
            recv_sem=rs2.at[q, sp],
            device_id=(j, dp),
            device_id_type=MESH,
        )

    def exchange_start(q, src, dst):
        def body(d, carry):
            exchange_copy(q, src, dst, d).start()
            return carry

        lax.fori_loop(1, SPAN, body, 0)

    def exchange_sent(q, src, dst):
        def body(d, carry):
            exchange_copy(q, src, dst, d).wait_send()
            return carry

        lax.fori_loop(1, SPAN, body, 0)

    def exchange_end(q, src, dst):
        def body(d, carry):
            i = (sp + d) % SPAN
            pltpu.make_async_remote_copy(
                src_ref=src(i),
                dst_ref=dst(i),
                send_sem=ss2.at[q, d],
                recv_sem=rs2.at[q, i],
                device_id=(i, dp),
                device_id_type=MESH,
            ).wait_recv()
            return carry

        lax.fori_loop(1, SPAN, body, 0)

    totals = (0, lambda j: tb, lambda i: tbuf.at[i])
    ends = (1, lambda j: xs.at[j // 2, j % 2], lambda i: rb.at[i])
    priors = (2, lambda j: ps.at[j], lambda i: pb.at[i // 2, i % 2])

    send(
        wcat.at[:, other], W.at[(slice(None), other, *here, core)], SHARDS, partner
    )
    send(
        act_hbm.at[pl.ds(ROWS - HALO, HALO)],
        act.at[pl.ds(0, HALO)],
        EDGE,
        ((sp + 1) % SPAN, dp),
    )
    load_w.wait()
    arrived(W.at[(slice(None), core, *here, other)], SHARDS)
    for color in range(3):
        one(ring_start, color)

    heads = lax.broadcasted_iota(jnp.int32, (16, WIDTH), 0)
    lanes = lax.broadcasted_iota(jnp.int32, (16, WIDTH), 1)
    expand = jnp.where(heads == lanes // 64, 1.0, 0.0).astype(BF16)
    load_act.wait()
    raw = rounded(dot(act[HALO : HALO + ROWS, :], rate_w[...])) + bias[...]
    rate_s[...] = jnp.maximum(raw, 0.0) + jnp.log1p(jnp.exp(-jnp.abs(raw)))

    for color in range(3):
        one(ring_pass, color)
    for color in range(3):
        one(ring_end, color)
    for stream in WAVES[0] + WAVES[1]:
        two(ring_start, stream)

    tri_r = lax.broadcasted_iota(jnp.int32, (BLOCK, BLOCK), 0)
    tri_c = lax.broadcasted_iota(jnp.int32, (BLOCK, BLOCK), 1)
    tri = jnp.where(tri_c <= tri_r, 1.0, 0.0).astype(BF16)
    decay = -jnp.exp(decay_log[...]) / LENGTH

    def fading(b, total):
        at = pl.ds(pl.multiple_of(b * BLOCK, BLOCK), BLOCK)
        rate = rate_s[at, :]
        running = sum(dot(tri, part) for part in split3(rate * decay))
        end = running[BLOCK - 1 : BLOCK, :]
        mid = 0.5 * end
        a = spread(jnp.exp(running - mid), expand)
        bb = spread(jnp.exp(mid - running) * rate, expand)
        for g in range(4):
            A[g, at, :] = a[:, g * 256 : g * 256 + 256]
            B[g, at, :] = bb[:, g * 256 : g * 256 + 256]
        EM[b] = spread(jnp.broadcast_to(jnp.exp(mid), (8, 16)), expand)
        return total + end

    total = lax.fori_loop(0, 4, fading, jnp.zeros((1, 16), F32))
    for stream in WAVES[0]:
        two(ring_pass, stream)
    total = lax.fori_loop(4, 8, fading, total)
    eye = jnp.where(
        lax.broadcasted_iota(jnp.int32, (16, 128), 0)
        == lax.broadcasted_iota(jnp.int32, (16, 128), 1),
        1.0,
        0.0,
    ).astype(BF16)
    tb[...] = spread(jnp.broadcast_to(total, (8, 16)), eye)
    tbuf[sp] = tb[...]
    for stream in WAVES[0]:
        two(ring_end, stream)
        three(ring_start, stream)
    for stream in WAVES[1]:
        two(ring_pass, stream)
    exchange_start(*totals)
    for stream in WAVES[1]:
        two(ring_end, stream)
    for stream in WAVES[2]:
        two(ring_start, stream)
    arrived(act.at[pl.ds(0, HALO)], EDGE)

    @pl.when(sp == 0)
    def _():
        act[0:HALO, :] = jnp.zeros((HALO, 2048), BF16)

    exchange_end(*totals)
    expand128 = jnp.where(
        lax.broadcasted_iota(jnp.int32, (128, WIDTH), 0)
        == lax.broadcasted_iota(jnp.int32, (128, WIDTH), 1) // 64,
        1.0,
        0.0,
    ).astype(BF16)
    factors = spread(jnp.exp(tbuf[...].reshape(128, 128)), expand128).reshape(SPAN, 8, WIDTH)
    D[0] = factors[:, :, :512]
    D[1] = factors[:, :, 512:]

    for stream in WAVES[0]:
        three(ring_pass, stream)
    for stream in WAVES[2]:
        two(ring_pass, stream)
    for stream in WAVES[1]:
        three(ring_start, stream)
    for stream in WAVES[2]:
        two(ring_end, stream)
    for stream in WAVES[0]:
        three(ring_end, stream)
        share(stream)

    def project(stream, cc):
        proj[...] = rounded(dot(act[...], W[stream, cc].reshape(2048, 256)))

    def convolved(at, taps):
        rows = proj[pl.ds(pl.multiple_of(at + 8, 8), 136), :]
        total = taps[3:4] * rows[8:136]
        for k in range(3):
            total = total + taps[k : k + 1] * rows[5 + k : 133 + k]
        return silu(total)

    def do_values(which, cc):
        g = 2 * which + cc
        project(VALUES[which], cc)
        taps = value_taps[:, g * 256 : g * 256 + 256].astype(F32)

        def body(i, carry):
            at = pl.multiple_of(i * 128, 128)
            v = rounded(convolved(at, taps))
            VB[g, pl.ds(at, 128), :] = (v * B[g, pl.ds(at, 128), :]).astype(BF16)
            return carry

        lax.fori_loop(0, 4, body, 0)

    def do_inputs(cc):
        project(INPUTS, cc)
        taps = input_taps[:, cc * 256 : cc * 256 + 256].astype(F32)

        def body(i, carry):
            at = pl.multiple_of(i * 128, 128)
            v = convolved(at, taps)
            for h in range(2):
                IT[2 * cc + h, :, pl.ds(at, 128)] = v[:, h * 128 : h * 128 + 128].T.astype(BF16)
            return carry

        lax.fori_loop(0, 4, body, 0)

    def do_reads(cc):
        project(READS, cc)
        taps = read_taps[:, cc * 256 : cc * 256 + 256].astype(F32)

        def body(i, carry):
            at = pl.multiple_of(i * 128, 128)
            v = convolved(at, taps).astype(BF16)
            for h in range(2):
                R[2 * cc + h, pl.ds(at, 128), :] = v[:, h * 128 : h * 128 + 128]
            return carry

        lax.fori_loop(0, 4, body, 0)

    def do_gate(which, cc):
        g = 2 * which + cc
        project(GATE[which], cc)

        def body(i, carry):
            at = pl.multiple_of(i * 128, 128)
            SG[g, pl.ds(at, 128), :] = silu(proj[pl.ds(at + HALO, 128), :])
            return carry

        lax.fori_loop(0, 4, body, 0)

    for stream in WAVES[0]:
        shared(stream)
    do_inputs(0)
    do_inputs(1)
    do_values(0, 0)
    for stream in WAVES[1]:
        three(ring_pass, stream)
    for stream in WAVES[2]:
        three(ring_start, stream)
    do_values(0, 1)
    do_values(1, 0)
    do_values(1, 1)

    def block_states(i, carry):
        at = pl.ds(pl.multiple_of(i * 128, 128), 128)
        zero = jnp.zeros((BLOCK, 256), BF16)
        for g in range(4):
            v = VB[g, at, :]
            both = jnp.concatenate(
                [
                    jnp.concatenate([v[:BLOCK], zero], axis=0),
                    jnp.concatenate([zero, v[BLOCK:]], axis=0),
                ],
                axis=1,
            )
            states = dot(IT[g, :, at], both)
            ST[g, 2 * i] = states[:, :256]
            ST[g, 2 * i + 1] = states[:, 256:]
        return carry

    lax.fori_loop(0, 4, block_states, 0)
    for stream in WAVES[1]:
        three(ring_end, stream)
        share(stream)
    for g in range(4):
        x = jnp.zeros((128, 256), F32)
        for b in range(8):
            em = EM[b, 0:1, g * 256 : g * 256 + 256]
            x = em * (em * x + ST[g, b])
        for n in range(8):
            xs[n, g // 2, :, (g % 2) * 256 : (g % 2) * 256 + 256] = x[n * 16 : n * 16 + 16].astype(
                BF16
            )
    exchange_start(*ends)
    keep = pltpu.make_async_copy(xs.at[sp // 2, sp % 2], rb.at[sp], ls.at[2])
    keep.start()
    for stream in WAVES[1]:
        shared(stream)
    do_reads(0)
    do_reads(1)
    for stream in WAVES[2]:
        three(ring_pass, stream)
    keep.wait()
    exchange_end(*ends)

    half = sp % 2

    def prefix(i, x):
        ps[i] = x.astype(BF16)
        return D[half, i][0:1, :] * x + rb[i].astype(F32)

    lax.fori_loop(0, SPAN, prefix, jnp.zeros((16, 512), F32))
    exchange_start(*priors)
    keep = pltpu.make_async_copy(ps.at[sp], pb.at[sp // 2, sp % 2], ls.at[2])
    keep.start()
    do_gate(0, 0)
    do_gate(0, 1)
    for stream in WAVES[2]:
        three(ring_end, stream)
        share(stream)
    do_gate(1, 0)
    do_gate(1, 1)
    keep.wait()
    exchange_end(*priors)
    for g in range(4):
        lane = (g % 2) * 256
        x = pb[:, g // 2, :, lane : lane + 256].reshape(128, 256).astype(F32)
        for b in range(8):
            em = EM[b, 0:1, g * 256 : g * 256 + 256]
            EN[g, b] = (em * x).astype(BF16)
            x = em * (em * x + ST[g, b])

    row = lax.broadcasted_iota(jnp.int32, (128, 128), 0)
    col = lax.broadcasted_iota(jnp.int32, (128, 128), 1)
    causal = (col <= row) & (row // BLOCK == col // BLOCK)

    def finish(i, carry):
        at = pl.ds(pl.multiple_of(i * 128, 128), 128)
        squares = jnp.zeros((128, 1), F32)
        for g in range(4):
            r = R[g, at, :]
            scores = jnp.where(causal, dot(r, IT[g, :, at]), 0.0).astype(BF16)
            across = jnp.concatenate(
                [dot(r[:BLOCK], EN[g, 2 * i]), dot(r[BLOCK:], EN[g, 2 * i + 1])], axis=0
            )
            mixed = A[g, at, :] * (dot(scores, VB[g, at, :]) + across)
            gated = rounded(mixed) * SG[g, at, :]
            GT[g] = gated
            squares = squares + jnp.sum(gated * gated, axis=1, keepdims=True)
        scale = lax.rsqrt(squares / WIDTH + 1.0)
        for g in range(4):
            lane = g * 256
            NORM[at, lane : lane + 256] = (GT[g] * scale * gain[:, lane : lane + 256]).astype(BF16)
        return carry

    lax.fori_loop(0, 4, finish, 0)
    for stream in WAVES[2]:
        shared(stream)

    def project_out(n, carry):
        w = jnp.concatenate(
            [
                W[OUT[q // 2], q % 2, n // 2, pl.ds((n % 2) * 2, 2)].reshape(256, 256)
                for q in range(4)
            ],
            axis=1,
        )
        tile = lax.dot_general(
            NORM[...], w, (((1,), (1,)), ((), ())), preferred_element_type=F32
        )
        out[:, pl.ds(pl.multiple_of(n * 256, 256), 256)] = tile.astype(BF16)
        return carry

    lax.fori_loop(0, 8, project_out, 0)

    for started in pending:
        started.wait_send()
    for q in (totals, ends, priors):
        exchange_sent(*q)


def per_device(
    activations,
    value_weight,
    gate_weight,
    input_weight,
    readout_weight,
    rate_weight,
    value_taps,
    input_taps,
    readout_taps,
    rate_bias,
    decay_log,
    norm_gain,
    out_weight,
):
    out_rows = out_weight.T
    streams = jnp.concatenate(
        [
            value_weight[:, :512],
            readout_weight,
            out_rows[:, :512],
            value_weight[:, 512:],
            gate_weight[:, :512],
            out_rows[:, 512:],
            input_weight,
            gate_weight[:, 512:],
        ],
        axis=1,
    )
    wcat = jnp.transpose(streams.reshape(16, 8, 2, 256), (1, 2, 0, 3))
    vmem = pl.BlockSpec(memory_space=pltpu.VMEM)
    result = pl.pallas_call(
        kernel,
        out_shape=jax.ShapeDtypeStruct((ROWS, 2048), BF16),
        in_specs=[pl.BlockSpec(memory_space=pl.ANY)] + [vmem] * 8,
        out_specs=vmem,
        scratch_shapes=[
            pltpu.VMEM((8, 2, 4, 4, 4, 2, 16, 256), BF16),
            pltpu.VMEM((HALO + ROWS, 2048), BF16),
            pltpu.VMEM((HALO + ROWS, 256), F32),
            pltpu.VMEM((ROWS, 16), F32),
            pltpu.VMEM((4, ROWS, 256), F32),
            pltpu.VMEM((4, ROWS, 256), F32),
            pltpu.VMEM((8, 8, WIDTH), F32),
            pltpu.VMEM((4, ROWS, 256), BF16),
            pltpu.VMEM((4, 128, ROWS), BF16),
            pltpu.VMEM((4, ROWS, 128), BF16),
            pltpu.VMEM((4, ROWS, 256), F32),
            pltpu.VMEM((4, 8, 128, 256), F32),
            pltpu.VMEM((4, 8, 128, 256), BF16),
            pltpu.VMEM((8, 128), F32),
            pltpu.VMEM((SPAN, 8, 128), F32),
            pltpu.VMEM((2, SPAN, 8, 512), F32),
            pltpu.VMEM((8, 2, 16, 512), BF16),
            pltpu.VMEM((SPAN, 16, 512), BF16),
            pltpu.VMEM((SPAN, 16, 512), BF16),
            pltpu.VMEM((8, 2, 16, 512), BF16),
            pltpu.VMEM((4, 128, 256), F32),
            pltpu.VMEM((ROWS, WIDTH), BF16),
            pltpu.SemaphoreType.DMA((86,)),
            pltpu.SemaphoreType.DMA((86,)),
            pltpu.SemaphoreType.DMA((3, SPAN)),
            pltpu.SemaphoreType.DMA((3, SPAN)),
            pltpu.SemaphoreType.DMA((3,)),
        ],
        compiler_params=pltpu.CompilerParams(
            collective_id=0, has_side_effects=True, vmem_limit_bytes=60 * 2**20
        ),
        name="mixer",
    )(
        activations[0],
        wcat,
        rate_weight,
        value_taps,
        input_taps,
        readout_taps,
        rate_bias[None],
        decay_log[None],
        norm_gain[None],
    )
    return result[None]


def solution(mesh):
    placed = (
        P("dp", "sp", None),
        P(("sp", "dp"), None),
        P(("sp", "dp"), None),
        P(("sp", "dp"), None),
        P(("sp", "dp"), None),
        P(),
        P(),
        P(),
        P(),
        P(),
        P(),
        P(),
        P(None, ("sp", "dp")),
    )
    return jax.shard_map(
        per_device, mesh=mesh, in_specs=placed, out_specs=P("dp", "sp", None), check_vma=False
    )
```

time: 258 us -> 96.8 us (0.38)
  waiting for transfers between devices: 121 us -> 0 us
  Pallas kernels: 0 us -> 84.7 us
  matrix products: 50.6 us -> 0 us
  local copies, waits for them, and re-layouts: 35.3 us -> 11.5 us
  other arithmetic: 18.1 us -> 0 us
  starting transfers between devices: 18.1 us -> 0 us
  between operations: 13.8 us -> 0.02 us
    pallas_call x0 -> x1, Pallas kernels: none -> 84.7 us  [per_device(): pl.pallas_call(kernel, out_shape=jax.ShapeDtypeStruct((ROWS, 2048), BF16)...]
    all_gather x2 -> x0, waiting for transfers between devices: 65.2 us -> none  [the longest x1 65.2 us: sent_together(): lax.all_gather(both, axis, axis=dim, tiled=True)]
    all_to_all x2 -> x0, waiting for transfers between devices: 55.6 us -> none  [sent_to_all(): return lax.all_to_all(copies, axis, split_axis=0, concat_axis=0, tiled=True)]
    dot_general x11 -> x0, matrix products: 50.6 us -> none  [the longest x4 17.3 us: add_rows(): return jnp.dot(sequence, piece, preferred_element_type=jnp.float32)]
    all_to_all x2 -> x0, starting transfers between devices: 14 us -> none  [sent_to_all(): return lax.all_to_all(copies, axis, split_axis=0, concat_axis=0, tiled=True)]
    convert_element_type x3 -> x0, local copies, waits for them, and re-layouts: 10.7 us -> none  [the longest x2 10.7 us: per_device(): returned.astype(jnp.float32) * jax.nn.silu(gate_proj.astype(jnp.float32))]
    another operation x3 -> x0, local copies, waits for them, and re-layouts: 7.45 us -> none  [the longest x2 6.79 us: block_parts(): block_values = values.reshape(blocks, BLOCK, head_count, head_width)]
    unnamed x50 -> x9, local copies, waits for them, and re-layouts: 4.43 us -> 10 us
  transfers between devices with their start and end apart: 5 -> 0, of which waited for: 2 -> 0; matrix products, arithmetic and copies ran while one was open for 34% -> 0% of each run, Pallas kernels for 0% -> 0%
where the time goes in v1:
time: 96.8 us; the launch traced here: 96.2 us
  Pallas kernels  84.7 us (88%)
  local copies, waits for them, and re-layouts  11.5 us (12%)
    pallas_call x1, Pallas kernels, per_device(): pl.pallas_call(kernel, out_shape=jax.ShapeDtypeStruct((ROWS, 2048), BF16)...  84.7 us
    unnamed x9, local copies, waits for them, and re-layouts  10 us

profile of v1, /device:TPU:0, one launch (start us, length us, event | category | flops | bytes accessed | tf_op | source)
XLA Modules:
  0.0 96.2 jit_solution(18264993296144592636)
XLA Ops:
  0.0 0.7 constant_dynamic-update-slice_fusion.7
  0.7 0.7 constant_dynamic-update-slice_fusion.6
  1.4 0.7 constant_dynamic-update-slice_fusion.5
  2.2 0.7 constant_dynamic-update-slice_fusion.4
  2.9 0.7 constant_dynamic-update-slice_fusion.3
  3.6 0.7 constant_dynamic-update-slice_fusion.2
  4.3 0.7 constant_dynamic-update-slice_fusion.1
  5.0 0.7 constant_dynamic-update-slice_fusion
  5.8 0.1 reshape.3
  5.8 0.7 copy.18
  6.5 1.8 %copy.16.rate_w = bf16[2048,16]{1,0:T(8,128)(2,1)} copy(bf16[2048,16]{0,1:T(8,128)(2,1)} %param.18) | data formatting | bytes 131072 | tf_op args[5]
  8.4 84.7 %mixer.1 = bf16[512,2048]{1,0:T(8,128)(2,1)} custom-call(bf16[512,2048]{1,0:T(8,128)(2,1)} %bitcast.10, bf16[8,2,16,256]{3,2,1,0:T(8,128)(2,1)} %bitcast.11, bf16[2048,16]{1,0:T(8,128)(2,1)} %copy.16.rate_w, bf16[4,1024]{1,0:T(4,128)(2,1)} %value_taps.1, bf16[4,512]{1,0:T(4,128)(2,1)} %input_taps.1, bf16[4,512]{1,0:T(4,128)(2,1)} %read_taps.1, ...), custom_call_target="tpu_custom_call" | custom-call | tf_op jit(solution)/shard_map/mixer/pallas_call | solution.py:554
  93.0 3.2 %copy.27 = bf16[1,512,2048]{2,1,0:T(8,128)(2,1)} copy(bf16[1,512,2048]{2,1,0:T(8,128)(2,1)} %bitcast.9) | data formatting | bytes 4194304

commit v2 on v1

v2 whole, which is shorter than its diff:
```python
import jax
import jax.numpy as jnp
from jax import lax
from jax.experimental import pallas as pl
from jax.experimental.pallas import tpu as pltpu
from jax.sharding import PartitionSpec as P

F32 = jnp.float32
BF16 = jnp.bfloat16
MESH = pl.DeviceIdType.MESH

ROWS = 512
HALO = 16
LENGTH = 8192
WIDTH = 1024
BLOCK = 64
SPAN = 16

ORDER = (("x", "y", "z"), ("z", "x", "y"), ("y", "z", "x"))
STREAMS = ((0, 3), (3, 3), (6, 2))
VALUES, INPUTS, READS, GATE, OUT = (0, 3), 6, 1, (4, 7), (2, 5)


def silu(v):
    return (0.5 * v) * (1.0 + jnp.tanh(0.5 * v))


def rounded(v):
    return v.astype(BF16).astype(F32)


def split3(x):
    hi = x.astype(BF16)
    rest = x - hi.astype(F32)
    mid = rest.astype(BF16)
    return hi, mid, (rest - mid.astype(F32)).astype(BF16)


def dot(a, b):
    return jnp.dot(a, b, preferred_element_type=F32)


def spread(x, m):
    return sum(dot(part, m) for part in split3(x))


def kernel(
    act_hbm,
    value_w,
    gate_w,
    input_w,
    read_w,
    out_w,
    rate_w,
    value_taps,
    input_taps,
    read_taps,
    bias,
    decay_log,
    gain,
    out,
    W,
    wcat,
    act,
    proj,
    rate_s,
    A,
    B,
    EM,
    VB,
    IT,
    R,
    SG,
    ST,
    EN,
    tb,
    tbuf,
    D,
    xs,
    rb,
    ps,
    pb,
    GT,
    NORM,
    ss,
    rs,
    ss2,
    rs2,
    ls,
    gs,
):
    sp = lax.axis_index("sp")
    dp = lax.axis_index("dp")
    c = {"z": sp // 4, "x": sp % 4, "y": dp // 2}
    core = dp % 2
    other = 1 - core
    partner = (sp, c["y"] * 2 + other)

    def neighbour(d, step, side=None):
        at = dict(c)
        at[d] = (c[d] + step) % 4
        return at["z"] * 4 + at["x"], at["y"] * 2 + (core if side is None else side)

    load_act = pltpu.make_async_copy(act_hbm, act.at[pl.ds(HALO, ROWS)], ls.at[0])
    load_act.start()
    here = (c["z"], c["x"], c["y"])
    shards = (
        (value_w, 0),
        (read_w, 0),
        (out_w, 0),
        (value_w, 512),
        (gate_w, 0),
        (out_w, 512),
        (input_w, 0),
        (gate_w, 512),
    )

    load_w = [
        pltpu.make_async_copy(ref.at[:, pl.ds(at, 512)], wcat.at[stream], ls.at[3 + stream])
        for stream, (ref, at) in enumerate(shards)
    ]
    for load in load_w:
        load.start()

    barrier = pltpu.get_barrier_semaphore()

    lines = [
        neighbour(d, step, side) for d in "xyz" for step in (1, 2, 3) for side in (core, other)
    ]
    for peer in lines + [partner]:
        pl.semaphore_signal(barrier, inc=1, device_id=peer, device_id_type=MESH)
    for load in load_w:
        load.wait()
    pl.semaphore_wait(barrier, 19)
    for step in (1, 2, 3):
        pl.semaphore_signal(gs, inc=1, device_id=neighbour("x", step), device_id_type=MESH)

    pending = []

    def copy(src, dst, sent, landed, device):
        return pltpu.make_async_remote_copy(
            src_ref=src,
            dst_ref=dst,
            send_sem=ss.at[sent],
            recv_sem=rs.at[landed],
            device_id=device,
            device_id_type=MESH,
        )

    def send(src, dst, k, device, landed=None):
        started = copy(src, dst, k, k if landed is None else landed, device)
        started.start()
        pending.append(started)

    def arrived(dst, k):
        copy(dst, dst, k, k, partner).wait_recv()

    def line_start(color):
        first, count = STREAMS[color]
        for t, step in enumerate((1, 3, 2)):
            for side in range(2):
                send(
                    wcat.at[first : first + count, :, side * 256 : side * 256 + 256],
                    W.at[(slice(first, first + count), side, *here, core)],
                    (color * 3 + t) * 2 + side,
                    neighbour(ORDER[color][0], step, side),
                    (color * 3 + t) * 2 + core,
                )

    def line_end(color):
        first, count = STREAMS[color]
        for t, step in enumerate((1, 3, 2)):
            at = dict(c)
            at[ORDER[color][0]] = (at[ORDER[color][0]] - step) % 4
            for side in range(2):
                arrived(
                    W.at[first : first + count, core, at["z"], at["x"], at["y"], side],
                    (color * 3 + t) * 2 + side,
                )

    def piece(phase, stream, index, half=None, side=None):
        dims = ORDER[stream // 3]
        at = dict(c)
        for d in dims[:phase]:
            at[d] = slice(None)
        at[dims[phase]] = index
        if half is not None:
            d = [d for d in "zxy" if d in dims[:phase]][0]
            at[d] = slice(2 * half, 2 * half + 2)
        return W.at[stream, core if side is None else side, at["z"], at["x"], at["y"]]

    def axis(phase, stream):
        d = ORDER[stream // 3][phase]
        return d, c[d], 18 + 48 * (phase - 1) + 6 * stream

    def ring_start(phase, stream, parts=(0, 1)):
        d, i, k = axis(phase, stream)
        halves = [piece(phase, stream, i, half) for half in range(2)]
        for j in parts:
            send(halves[j], halves[j], k + j, neighbour(d, 1))
            send(halves[1 - j], halves[1 - j], k + 2 + j, neighbour(d, 3))

    def ring_pass(phase, stream):
        d, i, k = axis(phase, stream)
        for side, (back, ahead) in enumerate(((3, 1), (1, 3))):
            half = piece(phase, stream, (i + back) % 4, side)
            arrived(half, k + 2 * side)
            send(half, half, k + 4 + side, neighbour(d, ahead))

    def ring_rest(phase, stream):
        d, i, k = axis(phase, stream)
        arrived(piece(phase, stream, (i + 3) % 4, 1), k + 1)
        arrived(piece(phase, stream, (i + 1) % 4, 0), k + 3)

    def ring_end(phase, stream):
        d, i, k = axis(phase, stream)
        for side in range(2):
            arrived(piece(phase, stream, (i + 2) % 4, side), k + 4 + side)

    def share(stream, step):
        i = (axis(2, stream)[1] + step) % 4
        plane = piece(2, stream, i)
        send(plane, plane, 114 + 4 * stream + step, partner)

    def shared(stream):
        for step in range(4):
            i = (axis(2, stream)[1] + step) % 4
            arrived(piece(2, stream, i, None, other), 114 + 4 * stream + step)

    def planes_start(streams):
        for stream in streams:
            ring_start(1, stream)

    def planes_pass(streams):
        for stream in streams:
            ring_pass(1, stream)

    def planes_end(streams):
        for stream in streams:
            ring_rest(1, stream)
            ring_end(1, stream)

    def cube_start(streams, parts=(0, 1)):
        for j in parts:
            for stream in streams:
                ring_start(2, stream, (j,))
                if j == 0:
                    share(stream, 0)

    def cube_pass(streams):
        for stream in streams:
            ring_pass(2, stream)

    def cube_rest(streams):
        for stream in streams:
            ring_rest(2, stream)
            share(stream, 1)
            share(stream, 3)

    def cube_end(streams):
        for stream in streams:
            ring_end(2, stream)
            share(stream, 2)

    def cube_shared(streams):
        for stream in streams:
            shared(stream)

    WAVES = ((6, 0, 3), (1, 4, 7), (2, 5))
    EDGE, GIVEN = 146, 147

    def exchange_copy(q, src, dst, d):
        j = (sp + d) % SPAN
        return pltpu.make_async_remote_copy(
            src_ref=src(j),
            dst_ref=dst(sp),
            send_sem=ss2.at[q, d],
            recv_sem=rs2.at[q, sp],
            device_id=(j, dp),
            device_id_type=MESH,
        )

    def exchange_start(q, src, dst):
        def body(d, carry):
            exchange_copy(q, src, dst, d).start()
            return carry

        lax.fori_loop(1, SPAN, body, 0)

    def exchange_sent(q, src, dst):
        def body(d, carry):
            exchange_copy(q, src, dst, d).wait_send()
            return carry

        lax.fori_loop(1, SPAN, body, 0)

    def exchange_end(q, src, dst):
        def body(d, carry):
            i = (sp + d) % SPAN
            pltpu.make_async_remote_copy(
                src_ref=src(i),
                dst_ref=dst(i),
                send_sem=ss2.at[q, d],
                recv_sem=rs2.at[q, i],
                device_id=(i, dp),
                device_id_type=MESH,
            ).wait_recv()
            return carry

        lax.fori_loop(1, SPAN, body, 0)

    totals = (0, lambda j: tb, lambda i: tbuf.at[i])
    ends = (1, lambda j: xs.at[j // 2, j % 2], lambda i: rb.at[i])
    priors = (2, lambda j: ps.at[j], lambda i: pb.at[i // 2, i % 2])

    for color in range(3):
        line_start(color)
    send(
        wcat.at[:, :, pl.ds(pl.multiple_of(other * 256, 256), 256)],
        W.at[(slice(None), other, *here, core)],
        GIVEN,
        partner,
    )
    keep_w = pltpu.make_async_copy(
        wcat.at[:, :, pl.ds(pl.multiple_of(core * 256, 256), 256)],
        W.at[(slice(None), core, *here, core)],
        ls.at[1],
    )
    keep_w.start()
    keep_w.wait()
    arrived(W.at[(slice(None), core, *here, other)], GIVEN)
    for color in range(3):
        line_end(color)
    planes_start(WAVES[0])
    planes_start(WAVES[1])
    pl.semaphore_wait(gs, 3)
    send(
        act_hbm.at[pl.ds(ROWS - HALO, HALO)],
        act.at[pl.ds(0, HALO)],
        EDGE,
        ((sp + 1) % SPAN, dp),
    )

    heads = lax.broadcasted_iota(jnp.int32, (16, WIDTH), 0)
    lanes = lax.broadcasted_iota(jnp.int32, (16, WIDTH), 1)
    expand = jnp.where(heads == lanes // 64, 1.0, 0.0).astype(BF16)
    load_act.wait()
    raw = lax.dot_general(
        act[HALO : HALO + ROWS, :],
        rate_w[...],
        (((1,), (1,)), ((), ())),
        preferred_element_type=F32,
    )
    raw = rounded(raw) + bias[...]
    rate_s[...] = jnp.maximum(raw, 0.0) + jnp.log1p(jnp.exp(-jnp.abs(raw)))

    tri_r = lax.broadcasted_iota(jnp.int32, (BLOCK, BLOCK), 0)
    tri_c = lax.broadcasted_iota(jnp.int32, (BLOCK, BLOCK), 1)
    tri = jnp.where(tri_c <= tri_r, 1.0, 0.0).astype(BF16)
    decay = -jnp.exp(decay_log[...]) / LENGTH

    def fading(b, total):
        at = pl.ds(pl.multiple_of(b * BLOCK, BLOCK), BLOCK)
        rate = rate_s[at, :]
        running = sum(dot(tri, part) for part in split3(rate * decay))
        end = running[BLOCK - 1 : BLOCK, :]
        mid = 0.5 * end
        a = spread(jnp.exp(running - mid), expand)
        bb = spread(jnp.exp(mid - running) * rate, expand)
        for g in range(4):
            A[g, at, :] = a[:, g * 256 : g * 256 + 256]
            B[g, at, :] = bb[:, g * 256 : g * 256 + 256]
        EM[b] = spread(jnp.broadcast_to(jnp.exp(mid), (8, 16)), expand)
        return total + end

    planes_pass(WAVES[0])
    total = lax.fori_loop(0, 3, fading, jnp.zeros((1, 16), F32))
    planes_end(WAVES[0])
    cube_start(WAVES[0])
    planes_pass(WAVES[1])
    total = lax.fori_loop(3, 6, fading, total)
    planes_start(WAVES[2])
    total = lax.fori_loop(6, 8, fading, total)
    eye = jnp.where(
        lax.broadcasted_iota(jnp.int32, (16, 128), 0)
        == lax.broadcasted_iota(jnp.int32, (16, 128), 1),
        1.0,
        0.0,
    ).astype(BF16)
    tb[...] = spread(jnp.broadcast_to(total, (8, 16)), eye)
    tbuf[sp] = tb[...]
    exchange_start(*totals)
    cube_pass(WAVES[0])
    planes_end(WAVES[1])
    cube_start(WAVES[1])
    planes_pass(WAVES[2])
    arrived(act.at[pl.ds(0, HALO)], EDGE)

    @pl.when(sp == 0)
    def _():
        act[0:HALO, :] = jnp.zeros((HALO, 2048), BF16)

    exchange_end(*totals)
    expand128 = jnp.where(
        lax.broadcasted_iota(jnp.int32, (128, WIDTH), 0)
        == lax.broadcasted_iota(jnp.int32, (128, WIDTH), 1) // 64,
        1.0,
        0.0,
    ).astype(BF16)
    factors = spread(jnp.exp(tbuf[...].reshape(128, 128)), expand128).reshape(SPAN, 8, WIDTH)
    D[0] = factors[:, :, :512]
    D[1] = factors[:, :, 512:]

    cube_rest(WAVES[0])
    planes_end(WAVES[2])
    cube_end(WAVES[0])

    def project(stream):
        w = jnp.concatenate([W[stream, cc].reshape(2048, 256) for cc in range(2)], axis=1)
        proj[...] = rounded(dot(act[...], w))

    def convolved(at, lane, taps):
        rows = proj[pl.ds(pl.multiple_of(at + 8, 8), 136), lane : lane + 256]
        total = taps[3:4] * rows[8:136]
        for k in range(3):
            total = total + taps[k : k + 1] * rows[5 + k : 133 + k]
        return silu(total)

    def over_rows(body):
        def step(i, carry):
            body(pl.multiple_of(i * 128, 128))
            return carry

        lax.fori_loop(0, 4, step, 0)

    def do_values(which):
        lane = which * 512
        taps = value_taps[:, lane : lane + 512].astype(F32)

        def body(at):
            for cc in range(2):
                v = rounded(convolved(at, cc * 256, taps[:, cc * 256 : cc * 256 + 256]))
                g = 2 * which + cc
                VB[g, pl.ds(at, 128), :] = (v * B[g, pl.ds(at, 128), :]).astype(BF16)

        over_rows(body)

    def do_inputs():
        taps = input_taps[...].astype(F32)

        def body(at):
            for cc in range(2):
                v = convolved(at, cc * 256, taps[:, cc * 256 : cc * 256 + 256])
                for h in range(2):
                    part = v[:, h * 128 : h * 128 + 128]
                    IT[2 * cc + h, :, pl.ds(at, 128)] = part.T.astype(BF16)

        over_rows(body)

    def do_reads():
        taps = read_taps[...].astype(F32)

        def body(at):
            for cc in range(2):
                v = convolved(at, cc * 256, taps[:, cc * 256 : cc * 256 + 256]).astype(BF16)
                for h in range(2):
                    R[2 * cc + h, pl.ds(at, 128), :] = v[:, h * 128 : h * 128 + 128]

        over_rows(body)

    def do_gate(which):
        def body(at):
            for cc in range(2):
                SG[2 * which + cc, pl.ds(at, 128), :] = silu(
                    proj[pl.ds(at + HALO, 128), cc * 256 : cc * 256 + 256]
                )

        over_rows(body)

    shared(INPUTS)
    project(INPUTS)
    cube_pass(WAVES[1])
    do_inputs()
    shared(VALUES[0])
    project(VALUES[0])
    do_values(0)
    cube_start(WAVES[2], (0,))
    cube_rest(WAVES[1])
    shared(VALUES[1])
    project(VALUES[1])
    do_values(1)

    def block_states(i, carry):
        at = pl.ds(pl.multiple_of(i * 128, 128), 128)
        zero = jnp.zeros((BLOCK, 256), BF16)
        for g in range(4):
            v = VB[g, at, :]
            both = jnp.concatenate(
                [
                    jnp.concatenate([v[:BLOCK], zero], axis=0),
                    jnp.concatenate([zero, v[BLOCK:]], axis=0),
                ],
                axis=1,
            )
            states = dot(IT[g, :, at], both)
            ST[g, 2 * i] = states[:, :256]
            ST[g, 2 * i + 1] = states[:, 256:]
        return carry

    lax.fori_loop(0, 4, block_states, 0)
    for g in range(4):
        x = jnp.zeros((128, 256), F32)
        for b in range(8):
            em = EM[b, 0:1, g * 256 : g * 256 + 256]
            x = em * (em * x + ST[g, b])
        for n in range(8):
            xs[n, g // 2, :, (g % 2) * 256 : (g % 2) * 256 + 256] = x[n * 16 : n * 16 + 16].astype(
                BF16
            )
    exchange_start(*ends)
    keep = pltpu.make_async_copy(xs.at[sp // 2, sp % 2], rb.at[sp], ls.at[2])
    keep.start()
    cube_start(WAVES[2], (1,))
    cube_end(WAVES[1])
    shared(READS)
    project(READS)
    cube_pass(WAVES[2])
    do_reads()
    shared(GATE[0])
    project(GATE[0])
    do_gate(0)
    cube_rest(WAVES[2])
    keep.wait()
    exchange_end(*ends)

    half = sp % 2

    def prefix(i, x):
        ps[i] = x.astype(BF16)
        return D[half, i][0:1, :] * x + rb[i].astype(F32)

    lax.fori_loop(0, SPAN, prefix, jnp.zeros((16, 512), F32))
    exchange_start(*priors)
    keep = pltpu.make_async_copy(ps.at[sp], pb.at[sp // 2, sp % 2], ls.at[2])
    keep.start()
    shared(GATE[1])
    project(GATE[1])
    do_gate(1)

    row = lax.broadcasted_iota(jnp.int32, (128, 128), 0)
    col = lax.broadcasted_iota(jnp.int32, (128, 128), 1)
    causal = (col <= row) & (row // BLOCK == col // BLOCK)

    def within(i, carry):
        at = pl.ds(pl.multiple_of(i * 128, 128), 128)
        for g in range(4):
            scores = jnp.where(causal, dot(R[g, at, :], IT[g, :, at]), 0.0).astype(BF16)
            B[g, at, :] = dot(scores, VB[g, at, :])
        return carry

    lax.fori_loop(0, 4, within, 0)
    cube_end(WAVES[2])
    keep.wait()
    exchange_end(*priors)
    for g in range(4):
        lane = (g % 2) * 256
        x = pb[:, g // 2, :, lane : lane + 256].reshape(128, 256).astype(F32)
        for b in range(8):
            em = EM[b, 0:1, g * 256 : g * 256 + 256]
            EN[g, b] = (em * x).astype(BF16)
            x = em * (em * x + ST[g, b])

    def finish(i, carry):
        at = pl.ds(pl.multiple_of(i * 128, 128), 128)
        squares = jnp.zeros((128, 1), F32)
        for g in range(4):
            r = R[g, at, :]
            across = jnp.concatenate(
                [dot(r[:BLOCK], EN[g, 2 * i]), dot(r[BLOCK:], EN[g, 2 * i + 1])], axis=0
            )
            mixed = A[g, at, :] * (B[g, at, :] + across)
            gated = rounded(mixed) * SG[g, at, :]
            GT[g] = gated
            squares = squares + jnp.sum(gated * gated, axis=1, keepdims=True)
        scale = lax.rsqrt(squares / WIDTH + 1.0)
        for g in range(4):
            lane = g * 256
            NORM[at, lane : lane + 256] = (GT[g] * scale * gain[:, lane : lane + 256]).astype(BF16)
        return carry

    lax.fori_loop(0, 4, finish, 0)
    cube_shared(WAVES[2])

    def project_out(n, carry):
        w = jnp.concatenate(
            [W[OUT[q // 2], q % 2, n].reshape(512, 256) for q in range(4)], axis=1
        )
        tile = lax.dot_general(
            NORM[...], w, (((1,), (1,)), ((), ())), preferred_element_type=F32
        )
        out[:, pl.ds(pl.multiple_of(n * 512, 512), 512)] = tile.astype(BF16)
        return carry

    lax.fori_loop(0, 4, project_out, 0)

    for started in pending:
        started.wait_send()
    for q in (totals, ends, priors):
        exchange_sent(*q)


def per_device(
    activations,
    value_weight,
    gate_weight,
    input_weight,
    readout_weight,
    rate_weight,
    value_taps,
    input_taps,
    readout_taps,
    rate_bias,
    decay_log,
    norm_gain,
    out_weight,
):
    vmem = pl.BlockSpec(memory_space=pltpu.VMEM)
    result = pl.pallas_call(
        kernel,
        out_shape=jax.ShapeDtypeStruct((ROWS, 2048), BF16),
        in_specs=[pl.BlockSpec(memory_space=pltpu.HBM)] * 6 + [vmem] * 7,
        out_specs=vmem,
        scratch_shapes=[
            pltpu.VMEM((8, 2, 4, 4, 4, 2, 16, 256), BF16),
            pltpu.VMEM((8, 16, 512), BF16),
            pltpu.VMEM((HALO + ROWS, 2048), BF16),
            pltpu.VMEM((HALO + ROWS, 512), F32),
            pltpu.VMEM((ROWS, 16), F32),
            pltpu.VMEM((4, ROWS, 256), F32),
            pltpu.VMEM((4, ROWS, 256), F32),
            pltpu.VMEM((8, 8, WIDTH), F32),
            pltpu.VMEM((4, ROWS, 256), BF16),
            pltpu.VMEM((4, 128, ROWS), BF16),
            pltpu.VMEM((4, ROWS, 128), BF16),
            pltpu.VMEM((4, ROWS, 256), F32),
            pltpu.VMEM((4, 8, 128, 256), F32),
            pltpu.VMEM((4, 8, 128, 256), BF16),
            pltpu.VMEM((8, 128), F32),
            pltpu.VMEM((SPAN, 8, 128), F32),
            pltpu.VMEM((2, SPAN, 8, 512), F32),
            pltpu.VMEM((8, 2, 16, 512), BF16),
            pltpu.VMEM((SPAN, 16, 512), BF16),
            pltpu.VMEM((SPAN, 16, 512), BF16),
            pltpu.VMEM((8, 2, 16, 512), BF16),
            pltpu.VMEM((4, 128, 256), F32),
            pltpu.VMEM((ROWS, WIDTH), BF16),
            pltpu.SemaphoreType.DMA((148,)),
            pltpu.SemaphoreType.DMA((148,)),
            pltpu.SemaphoreType.DMA((3, SPAN)),
            pltpu.SemaphoreType.DMA((3, SPAN)),
            pltpu.SemaphoreType.DMA((11,)),
            pltpu.SemaphoreType.REGULAR,
        ],
        compiler_params=pltpu.CompilerParams(
            collective_id=0, has_side_effects=True, vmem_limit_bytes=58 * 2**20
        ),
        name="mixer",
    )(
        activations[0],
        value_weight,
        gate_weight,
        input_weight,
        readout_weight,
        out_weight.T,
        rate_weight.T,
        value_taps,
        input_taps,
        readout_taps,
        rate_bias[None],
        decay_log[None],
        norm_gain[None],
    )
    return result[None]


def solution(mesh):
    placed = (
        P("dp", "sp", None),
        P(("sp", "dp"), None),
        P(("sp", "dp"), None),
        P(("sp", "dp"), None),
        P(("sp", "dp"), None),
        P(),
        P(),
        P(),
        P(),
        P(),
        P(),
        P(),
        P(None, ("sp", "dp")),
    )
    return jax.shard_map(
        per_device, mesh=mesh, in_specs=placed, out_specs=P("dp", "sp", None), check_vma=False
    )
```

time: 96.8 us -> 76.6 us (0.79)
  Pallas kernels: 84.7 us -> 72.2 us
  local copies, waits for them, and re-layouts: 11.5 us -> 3.16 us
    pallas_call x1, Pallas kernels: 84.7 us -> 72.2 us  [per_device(): pl.pallas_call(kernel, out_shape=jax.ShapeDtypeStruct((ROWS, 2048), BF16)...]
    unnamed x9 -> x1, local copies, waits for them, and re-layouts: 10 us -> 3.16 us
where the time goes in v2:
time: 76.6 us; the launch traced here: 75.4 us
  Pallas kernels  72.2 us (94%)
  local copies, waits for them, and re-layouts  3.16 us (4%)
    pallas_call x1, Pallas kernels, per_device(): pl.pallas_call(kernel, out_shape=jax.ShapeDtypeStruct((ROWS, 2048), BF16)...  72.2 us
    unnamed x1, local copies, waits for them, and re-layouts  3.16 us

profile of v2, /device:TPU:0, one launch (start us, length us, event | category | flops | bytes accessed | tf_op | source)
XLA Modules:
  0.0 75.4 jit_solution(15157309921068053665)
XLA Ops:
  0.0 72.2 %mixer.1 = bf16[512,2048]{1,0:T(8,128)(2,1)} custom-call(bf16[512,2048]{1,0:T(8,128)(2,1)} %bitcast.8, bf16[16,1024]{1,0:T(8,128)(2,1)} %value_w.1, bf16[16,1024]{1,0:T(8,128)(2,1)} %gate_w.1, bf16[16,512]{1,0:T(8,128)(2,1)} %input_w.1, bf16[16,512]{1,0:T(8,128)(2,1)} %read_w.1, bf16[16,1024]{1,0:T(8,128)(2,1)} %bitcast.10, bf16[16,2048]{1,0:T(8,128)(2,1)} %bitcast.9, ...), custom_call_target="tpu_custom_call" | custom-call | tf_op jit(solution)/shard_map/mixer/pallas_call | solution.py:628
  72.2 3.2 %copy.15 = bf16[1,512,2048]{2,1,0:T(8,128)(2,1)} copy(bf16[1,512,2048]{2,1,0:T(8,128)(2,1)} %bitcast.7) | data formatting | bytes 4194304

commit v3 on v2

--- a/solution.py
+++ b/solution.py
@@ -51,6 +51,14 @@
     input_w,
     read_w,
     out_w,
+    rate_w_hbm,
+    value_taps_hbm,
+    input_taps_hbm,
+    read_taps_hbm,
+    bias_hbm,
+    decay_log_hbm,
+    gain_hbm,
+    out,
     rate_w,
     value_taps,
     input_taps,
@@ -58,7 +66,6 @@
     bias,
     decay_log,
     gain,
-    out,
     W,
     wcat,
     act,
@@ -84,8 +91,6 @@
     NORM,
     ss,
     rs,
-    ss2,
-    rs2,
     ls,
     gs,
 ):
@@ -101,8 +106,27 @@
         at[d] = (c[d] + step) % 4
         return at["z"] * 4 + at["x"], at["y"] * 2 + (core if side is None else side)
 
+    barrier = pltpu.get_barrier_semaphore()
+
+    lines = [
+        neighbour(d, step, side) for d in "xyz" for step in (1, 2, 3) for side in (core, other)
+    ]
+    for peer in lines + [partner]:
+        pl.semaphore_signal(barrier, inc=1, device_id=peer, device_id_type=MESH)
+
+    small = (
+        (rate_w_hbm, rate_w),
+        (value_taps_hbm, value_taps),
+        (input_taps_hbm, input_taps),
+        (read_taps_hbm, read_taps),
+        (bias_hbm, bias),
+        (decay_log_hbm, decay_log),
+        (gain_hbm, gain),
+    )
+    load_small = [
+        pltpu.make_async_copy(src, dst, ls.at[4 + n]) for n, (src, dst) in enumerate(small)
+    ]
     load_act = pltpu.make_async_copy(act_hbm, act.at[pl.ds(HALO, ROWS)], ls.at[0])
-    load_act.start()
     here = (c["z"], c["x"], c["y"])
     shards = (
         (value_w, 0),
@@ -116,67 +140,53 @@
     )
 
     load_w = [
-        pltpu.make_async_copy(ref.at[:, pl.ds(at, 512)], wcat.at[stream], ls.at[3 + stream])
+        pltpu.make_async_copy(ref.at[:, pl.ds(at, 512)], wcat.at[stream], ls.at[3])
         for stream, (ref, at) in enumerate(shards)
     ]
-    for load in load_w:
+    for load in [*load_w, load_act, *load_small]:
         load.start()
-
-    barrier = pltpu.get_barrier_semaphore()
-
-    lines = [
-        neighbour(d, step, side) for d in "xyz" for step in (1, 2, 3) for side in (core, other)
-    ]
-    for peer in lines + [partner]:
-        pl.semaphore_signal(barrier, inc=1, device_id=peer, device_id_type=MESH)
-    for load in load_w:
-        load.wait()
+    pltpu.make_async_copy(wcat, wcat, ls.at[3]).wait()
     pl.semaphore_wait(barrier, 19)
     for step in (1, 2, 3):
         pl.semaphore_signal(gs, inc=1, device_id=neighbour("x", step), device_id_type=MESH)
 
-    pending = []
-
-    def copy(src, dst, sent, landed, device):
-        return pltpu.make_async_remote_copy(
+    sent = []
+
+    def send(src, dst, units, k, device):
+        pltpu.make_async_remote_copy(
             src_ref=src,
             dst_ref=dst,
-            send_sem=ss.at[sent],
-            recv_sem=rs.at[landed],
+            send_sem=ss.at[0],
+            recv_sem=rs.at[k],
             device_id=device,
             device_id_type=MESH,
-        )
-
-    def send(src, dst, k, device, landed=None):
-        started = copy(src, dst, k, k if landed is None else landed, device)
-        started.start()
-        pending.append(started)
-
-    def arrived(dst, k):
-        copy(dst, dst, k, k, partner).wait_recv()
-
-    def line_start(color):
-        first, count = STREAMS[color]
+        ).start()
+        sent.append(units)
+
+    def landed(view, k):
+        pltpu.make_async_remote_copy(
+            src_ref=view,
+            dst_ref=view,
+            send_sem=ss.at[0],
+            recv_sem=rs.at[k],
+            device_id=partner,
+            device_id_type=MESH,
+        ).wait_recv()
+
+    def line_start(wave):
         for t, step in enumerate((1, 3, 2)):
-            for side in range(2):
-                send(
-                    wcat.at[first : first + count, :, side * 256 : side * 256 + 256],
-                    W.at[(slice(first, first + count), side, *here, core)],
-                    (color * 3 + t) * 2 + side,
-                    neighbour(ORDER[color][0], step, side),
-                    (color * 3 + t) * 2 + core,
-                )
-
-    def line_end(color):
-        first, count = STREAMS[color]
-        for t, step in enumerate((1, 3, 2)):
-            at = dict(c)
-            at[ORDER[color][0]] = (at[ORDER[color][0]] - step) % 4
-            for side in range(2):
-                arrived(
-                    W.at[first : first + count, core, at["z"], at["x"], at["y"], side],
-                    (color * 3 + t) * 2 + side,
-                )
+            for stream in WAVES[wave]:
+                for side in range(2):
+                    send(
+                        wcat.at[stream, :, side * 256 : side * 256 + 256],
+                        W.at[(stream, side, *here, core)],
+                        1,
+                        wave,
+                        neighbour(ORDER[stream // 3][0], step, side),
+                    )
+
+    def line_end(wave):
+        landed(W.at[0 : len(WAVES[wave]), core, 0, 0, 0:3], wave)
 
     def piece(phase, stream, index, half=None, side=None):
         dims = ORDER[stream // 3]
@@ -191,133 +201,114 @@
 
     def axis(phase, stream):
         d = ORDER[stream // 3][phase]
-        return d, c[d], 18 + 48 * (phase - 1) + 6 * stream
-
-    def ring_start(phase, stream, parts=(0, 1)):
-        d, i, k = axis(phase, stream)
-        halves = [piece(phase, stream, i, half) for half in range(2)]
-        for j in parts:
-            send(halves[j], halves[j], k + j, neighbour(d, 1))
-            send(halves[1 - j], halves[1 - j], k + 2 + j, neighbour(d, 3))
-
-    def ring_pass(phase, stream):
-        d, i, k = axis(phase, stream)
-        for side, (back, ahead) in enumerate(((3, 1), (1, 3))):
-            half = piece(phase, stream, (i + back) % 4, side)
-            arrived(half, k + 2 * side)
-            send(half, half, k + 4 + side, neighbour(d, ahead))
-
-    def ring_rest(phase, stream):
-        d, i, k = axis(phase, stream)
-        arrived(piece(phase, stream, (i + 3) % 4, 1), k + 1)
-        arrived(piece(phase, stream, (i + 1) % 4, 0), k + 3)
-
-    def ring_end(phase, stream):
-        d, i, k = axis(phase, stream)
-        for side in range(2):
-            arrived(piece(phase, stream, (i + 2) % 4, side), k + 4 + side)
-
-    def share(stream, step):
-        i = (axis(2, stream)[1] + step) % 4
-        plane = piece(2, stream, i)
-        send(plane, plane, 114 + 4 * stream + step, partner)
+        return d, c[d]
+
+    def ring_start(phase, stream, k, units, part):
+        d, i = axis(phase, stream)
+        for half, near, far in ((part, k, k + 1), (1 - part, k, k + 1)):
+            ahead = 1 if half == part else 3
+            own = piece(phase, stream, i, half)
+            send(own, own, units, near if part == 0 else far, neighbour(d, ahead))
+
+    def ring_pass(phase, stream, k, units):
+        d, i = axis(phase, stream)
+        for half, back, ahead in ((0, 3, 1), (1, 1, 3)):
+            block = piece(phase, stream, (i + back) % 4, half)
+            send(block, block, units, k, neighbour(d, ahead))
+
+    def share(stream, step, half):
+        block = piece(2, stream, (axis(2, stream)[1] + step) % 4, half)
+        send(block, block, 16, 33 + stream, partner)
 
     def shared(stream):
-        for step in range(4):
-            i = (axis(2, stream)[1] + step) % 4
-            arrived(piece(2, stream, i, None, other), 114 + 4 * stream + step)
-
-    def planes_start(streams):
-        for stream in streams:
-            ring_start(1, stream)
-
-    def planes_pass(streams):
-        for stream in streams:
-            ring_pass(1, stream)
-
-    def planes_end(streams):
-        for stream in streams:
-            ring_rest(1, stream)
-            ring_end(1, stream)
-
-    def cube_start(streams, parts=(0, 1)):
-        for j in parts:
-            for stream in streams:
-                ring_start(2, stream, (j,))
-                if j == 0:
-                    share(stream, 0)
-
-    def cube_pass(streams):
-        for stream in streams:
-            ring_pass(2, stream)
-
-    def cube_rest(streams):
-        for stream in streams:
-            ring_rest(2, stream)
-            share(stream, 1)
-            share(stream, 3)
-
-    def cube_end(streams):
-        for stream in streams:
-            ring_end(2, stream)
-            share(stream, 2)
-
-    def cube_shared(streams):
-        for stream in streams:
+        landed(W.at[stream, other], 33 + stream)
+
+    def planes_start(wave):
+        for part in range(2):
+            for stream in WAVES[wave]:
+                ring_start(1, stream, 3 + 2 * wave, 4, part)
+
+    def planes_pass(wave):
+        landed(W.at[0 : len(WAVES[wave]), core, 0, 0], 3 + 2 * wave)
+        for stream in WAVES[wave]:
+            ring_pass(1, stream, 4 + 2 * wave, 4)
+
+    def planes_end(wave):
+        landed(W.at[0 : len(WAVES[wave]), core, 0, 0:2], 4 + 2 * wave)
+
+    def cube_start(wave, parts=(0, 1)):
+        for part in parts:
+            for stream in WAVES[wave]:
+                ring_start(2, stream, 9 + 3 * stream, 16, part)
+                share(stream, 0, part)
+
+    def cube_pass(wave):
+        for stream in WAVES[wave]:
+            landed(W.at[stream, core, 0], 9 + 3 * stream)
+            ring_pass(2, stream, 11 + 3 * stream, 16)
+            share(stream, 3, 0)
+            share(stream, 1, 1)
+
+    def cube_rest(wave):
+        for stream in WAVES[wave]:
+            landed(W.at[stream, core, 0], 10 + 3 * stream)
+            share(stream, 3, 1)
+            share(stream, 1, 0)
+
+    def cube_end(wave):
+        for stream in WAVES[wave]:
+            landed(W.at[stream, core, 0], 11 + 3 * stream)
+            share(stream, 2, 0)
+            share(stream, 2, 1)
+
+    def cube_shared(wave):
+        for stream in WAVES[wave]:
             shared(stream)
 
     WAVES = ((6, 0, 3), (1, 4, 7), (2, 5))
-    EDGE, GIVEN = 146, 147
-
-    def exchange_copy(q, src, dst, d):
-        j = (sp + d) % SPAN
+    EDGE, GIVEN = 41, 42
+
+    def exchange_start(q, src, dst, slots):
+        def body(d, carry):
+            j = (sp + d) % SPAN
+            pltpu.make_async_remote_copy(
+                src_ref=src(j),
+                dst_ref=dst(sp),
+                send_sem=ss.at[1 + q],
+                recv_sem=rs.at[43 + q],
+                device_id=(j, dp),
+                device_id_type=MESH,
+            ).start()
+            return carry
+
+        lax.fori_loop(1, SPAN, body, 0)
+
+    def exchange_all(q, slots):
+        view = slots.at[0 : SPAN - 1]
         return pltpu.make_async_remote_copy(
-            src_ref=src(j),
-            dst_ref=dst(sp),
-            send_sem=ss2.at[q, d],
-            recv_sem=rs2.at[q, sp],
-            device_id=(j, dp),
+            src_ref=view,
+            dst_ref=view,
+            send_sem=ss.at[1 + q],
+            recv_sem=rs.at[43 + q],
+            device_id=partner,
             device_id_type=MESH,
         )
 
-    def exchange_start(q, src, dst):
-        def body(d, carry):
-            exchange_copy(q, src, dst, d).start()
-            return carry
-
-        lax.fori_loop(1, SPAN, body, 0)
-
-    def exchange_sent(q, src, dst):
-        def body(d, carry):
-            exchange_copy(q, src, dst, d).wait_send()
-            return carry
-
-        lax.fori_loop(1, SPAN, body, 0)
-
-    def exchange_end(q, src, dst):
-        def body(d, carry):
-            i = (sp + d) % SPAN
-            pltpu.make_async_remote_copy(
-                src_ref=src(i),
-                dst_ref=dst(i),
-                send_sem=ss2.at[q, d],
-                recv_sem=rs2.at[q, i],
-                device_id=(i, dp),
-                device_id_type=MESH,
-            ).wait_recv()
-            return carry
-
-        lax.fori_loop(1, SPAN, body, 0)
-
-    totals = (0, lambda j: tb, lambda i: tbuf.at[i])
-    ends = (1, lambda j: xs.at[j // 2, j % 2], lambda i: rb.at[i])
-    priors = (2, lambda j: ps.at[j], lambda i: pb.at[i // 2, i % 2])
-
-    for color in range(3):
-        line_start(color)
+    def exchange_end(q, src, dst, slots):
+        exchange_all(q, slots).wait_recv()
+
+    def exchange_sent(q, src, dst, slots):
+        exchange_all(q, slots).wait_send()
+
+    totals = (0, lambda j: tb, lambda i: tbuf.at[i], tbuf)
+    ends = (1, lambda j: xs.at[j // 2, j % 2], lambda i: rb.at[i], rb)
+    priors = (2, lambda j: ps.at[j], lambda i: pb.at[i // 2, i % 2], ps)
+
+    line_start(0)
     send(
         wcat.at[:, :, pl.ds(pl.multiple_of(other * 256, 256), 256)],
         W.at[(slice(None), other, *here, core)],
+        8,
         GIVEN,
         partner,
     )
@@ -327,16 +318,19 @@
         ls.at[1],
     )
     keep_w.start()
+    line_start(1)
     keep_w.wait()
-    arrived(W.at[(slice(None), core, *here, other)], GIVEN)
-    for color in range(3):
-        line_end(color)
-    planes_start(WAVES[0])
-    planes_start(WAVES[1])
+    landed(W.at[(slice(None), core, *here, other)], GIVEN)
+    line_end(0)
+    planes_start(0)
+    line_start(2)
+    line_end(1)
+    planes_start(1)
     pl.semaphore_wait(gs, 3)
     send(
         act_hbm.at[pl.ds(ROWS - HALO, HALO)],
         act.at[pl.ds(0, HALO)],
+        8,
         EDGE,
         ((sp + 1) % SPAN, dp),
     )
@@ -345,6 +339,8 @@
     lanes = lax.broadcasted_iota(jnp.int32, (16, WIDTH), 1)
     expand = jnp.where(heads == lanes // 64, 1.0, 0.0).astype(BF16)
     load_act.wait()
+    for load in load_small:
+        load.wait()
     raw = lax.dot_general(
         act[HALO : HALO + ROWS, :],
         rate_w[...],
@@ -373,14 +369,14 @@
         EM[b] = spread(jnp.broadcast_to(jnp.exp(mid), (8, 16)), expand)
         return total + end
 
-    planes_pass(WAVES[0])
-    total = lax.fori_loop(0, 3, fading, jnp.zeros((1, 16), F32))
-    planes_end(WAVES[0])
-    cube_start(WAVES[0])
-    planes_pass(WAVES[1])
-    total = lax.fori_loop(3, 6, fading, total)
-    planes_start(WAVES[2])
-    total = lax.fori_loop(6, 8, fading, total)
+    planes_pass(0)
+    line_end(2)
+    total = lax.fori_loop(0, 2, fading, jnp.zeros((1, 16), F32))
+    planes_pass(1)
+    planes_end(0)
+    cube_start(0)
+    planes_start(2)
+    total = lax.fori_loop(2, 8, fading, total)
     eye = jnp.where(
         lax.broadcasted_iota(jnp.int32, (16, 128), 0)
         == lax.broadcasted_iota(jnp.int32, (16, 128), 1),
@@ -390,30 +386,18 @@
     tb[...] = spread(jnp.broadcast_to(total, (8, 16)), eye)
     tbuf[sp] = tb[...]
     exchange_start(*totals)
-    cube_pass(WAVES[0])
-    planes_end(WAVES[1])
-    cube_start(WAVES[1])
-    planes_pass(WAVES[2])
-    arrived(act.at[pl.ds(0, HALO)], EDGE)
+    cube_pass(0)
+    planes_end(1)
+    cube_start(1)
+    planes_pass(2)
+    landed(act.at[pl.ds(0, HALO)], EDGE)
 
     @pl.when(sp == 0)
     def _():
         act[0:HALO, :] = jnp.zeros((HALO, 2048), BF16)
 
-    exchange_end(*totals)
-    expand128 = jnp.where(
-        lax.broadcasted_iota(jnp.int32, (128, WIDTH), 0)
-        == lax.broadcasted_iota(jnp.int32, (128, WIDTH), 1) // 64,
-        1.0,
-        0.0,
-    ).astype(BF16)
-    factors = spread(jnp.exp(tbuf[...].reshape(128, 128)), expand128).reshape(SPAN, 8, WIDTH)
-    D[0] = factors[:, :, :512]
-    D[1] = factors[:, :, 512:]
-
-    cube_rest(WAVES[0])
-    planes_end(WAVES[2])
-    cube_end(WAVES[0])
+    cube_rest(0)
+    cube_end(0)
 
     def project(stream):
         w = jnp.concatenate([W[stream, cc].reshape(2048, 256) for cc in range(2)], axis=1)
@@ -479,15 +463,16 @@
 
     shared(INPUTS)
     project(INPUTS)
-    cube_pass(WAVES[1])
     do_inputs()
     shared(VALUES[0])
     project(VALUES[0])
+    cube_pass(1)
+    planes_end(2)
+    cube_start(2, (0,))
     do_values(0)
-    cube_start(WAVES[2], (0,))
-    cube_rest(WAVES[1])
     shared(VALUES[1])
     project(VALUES[1])
+    cube_rest(1)
     do_values(1)
 
     def block_states(i, carry):
@@ -520,16 +505,23 @@
     exchange_start(*ends)
     keep = pltpu.make_async_copy(xs.at[sp // 2, sp % 2], rb.at[sp], ls.at[2])
     keep.start()
-    cube_start(WAVES[2], (1,))
-    cube_end(WAVES[1])
+    cube_start(2, (1,))
+    cube_end(1)
+    exchange_end(*totals)
+    expand128 = jnp.where(
+        lax.broadcasted_iota(jnp.int32, (128, WIDTH), 0)
+        == lax.broadcasted_iota(jnp.int32, (128, WIDTH), 1) // 64,
+        1.0,
+        0.0,
+    ).astype(BF16)
+    factors = spread(jnp.exp(tbuf[...].reshape(128, 128)), expand128).reshape(SPAN, 8, WIDTH)
+    D[0] = factors[:, :, :512]
+    D[1] = factors[:, :, 512:]
+
     shared(READS)
     project(READS)
-    cube_pass(WAVES[2])
+    cube_pass(2)
     do_reads()
-    shared(GATE[0])
-    project(GATE[0])
-    do_gate(0)
-    cube_rest(WAVES[2])
     keep.wait()
     exchange_end(*ends)
 
@@ -543,6 +535,9 @@
     exchange_start(*priors)
     keep = pltpu.make_async_copy(ps.at[sp], pb.at[sp // 2, sp % 2], ls.at[2])
     keep.start()
+    shared(GATE[0])
+    project(GATE[0])
+    do_gate(0)
     shared(GATE[1])
     project(GATE[1])
     do_gate(1)
@@ -559,7 +554,8 @@
         return carry
 
     lax.fori_loop(0, 4, within, 0)
-    cube_end(WAVES[2])
+    cube_rest(2)
+    cube_end(2)
     keep.wait()
     exchange_end(*priors)
     for g in range(4):
@@ -589,7 +585,7 @@
         return carry
 
     lax.fori_loop(0, 4, finish, 0)
-    cube_shared(WAVES[2])
+    cube_shared(2)
 
     def project_out(n, carry):
         w = jnp.concatenate(
@@ -603,8 +599,15 @@
 
     lax.fori_loop(0, 4, project_out, 0)
 
-    for started in pending:
-        started.wait_send()
+    assert sum(sent) == 2048
+    pltpu.make_async_remote_copy(
+        src_ref=W,
+        dst_ref=W,
+        send_sem=ss.at[0],
+        recv_sem=rs.at[0],
+        device_id=partner,
+        device_id_type=MESH,
+    ).wait_send()
     for q in (totals, ends, priors):
         exchange_sent(*q)
 
@@ -624,13 +627,20 @@
     norm_gain,
     out_weight,
 ):
-    vmem = pl.BlockSpec(memory_space=pltpu.VMEM)
+    hbm = pl.BlockSpec(memory_space=pltpu.HBM)
     result = pl.pallas_call(
         kernel,
-        out_shape=jax.ShapeDtypeStruct((ROWS, 2048), BF16),
-        in_specs=[pl.BlockSpec(memory_space=pltpu.HBM)] * 6 + [vmem] * 7,
-        out_specs=vmem,
+        out_shape=pltpu.VMEM((ROWS, 2048), BF16),
+        in_specs=[hbm] * 13,
+        out_specs=pl.BlockSpec(memory_space=pltpu.VMEM),
         scratch_shapes=[
+            pltpu.VMEM((16, 2048), BF16),
+            pltpu.VMEM((4, 1024), BF16),
+            pltpu.VMEM((4, 512), BF16),
+            pltpu.VMEM((4, 512), BF16),
+            pltpu.VMEM((1, 16), F32),
+            pltpu.VMEM((1, 16), F32),
+            pltpu.VMEM((1, WIDTH), F32),
             pltpu.VMEM((8, 2, 4, 4, 4, 2, 16, 256), BF16),
             pltpu.VMEM((8, 16, 512), BF16),
             pltpu.VMEM((HALO + ROWS, 2048), BF16),
@@ -654,10 +664,8 @@
             pltpu.VMEM((8, 2, 16, 512), BF16),
             pltpu.VMEM((4, 128, 256), F32),
             pltpu.VMEM((ROWS, WIDTH), BF16),
-            pltpu.SemaphoreType.DMA((148,)),
-            pltpu.SemaphoreType.DMA((148,)),
-            pltpu.SemaphoreType.DMA((3, SPAN)),
-            pltpu.SemaphoreType.DMA((3, SPAN)),
+            pltpu.SemaphoreType.DMA((4,)),
+            pltpu.SemaphoreType.DMA((46,)),
             pltpu.SemaphoreType.DMA((11,)),
             pltpu.SemaphoreType.REGULAR,
         ],

time: 76.6 us -> 62.9 us (0.82)
  Pallas kernels: 72.2 us -> 61 us
  local copies, waits for them, and re-layouts: 3.16 us -> 1.32 us
    pallas_call x1, Pallas kernels: 72.2 us -> 61 us  [per_device(): pl.pallas_call(kernel, out_shape=pltpu.VMEM((ROWS, 2048), BF16), in_specs...]
    unnamed x1, local copies, waits for them, and re-layouts: 3.16 us -> 1.32 us
where the time goes in v3:
time: 62.9 us; the launch traced here: 62.4 us
  Pallas kernels  61 us (97%)
  local copies, waits for them, and re-layouts  1.32 us (2%)
    pallas_call x1, Pallas kernels, per_device(): pl.pallas_call(kernel, out_shape=pltpu.VMEM((ROWS, 2048), BF16), in_specs...  61 us
    unnamed x1, local copies, waits for them, and re-layouts  1.32 us

profile of v3, /device:TPU:0, one launch (start us, length us, event | category | flops | bytes accessed | tf_op | source)
XLA Modules:
  0.0 62.4 jit_solution(10705373393551364215)
XLA Ops:
  0.0 61.0 %mixer.1 = bf16[512,2048]{1,0:T(8,128)(2,1)S(1)} custom-call(bf16[512,2048]{1,0:T(8,128)(2,1)} %bitcast.8, bf16[16,1024]{1,0:T(8,128)(2,1)} %value_w.1, bf16[16,1024]{1,0:T(8,128)(2,1)} %gate_w.1, bf16[16,512]{1,0:T(8,128)(2,1)} %input_w.1, bf16[16,512]{1,0:T(8,128)(2,1)} %read_w.1, bf16[16,1024]{1,0:T(8,128)(2,1)} %bitcast.10, bf16[16,2048]{1,0:T(8,128)(2,1)} %bitcast.9, ...), custom_call_target="tpu_custom_call" | custom-call | tf_op jit(solution)/shard_map/mixer/pallas_call | solution.py:631
  61.0 1.3 %copy.15 = bf16[1,512,2048]{2,1,0:T(8,128)(2,1)} copy(bf16[1,512,2048]{2,1,0:T(8,128)(2,1)S(1)} %bitcast.7) | data formatting | bytes 4194304
